TPU v7x, 32 devices: a whole 2x2x4 slice. The times are simulated.
32 devices in a mesh: sp: 8 (over z, core), tp: 4 (over y, x).
Axes of the slice: x: 2, y: 2, z: 4, core: 2. Of those that a mesh axis runs over, the one named last changes fastest.
Arguments:
- moe_input: bfloat16 [1024, 2048], P('sp', 'tp'), may hold values from -6 to 6
- cotangent: bfloat16 [1024, 2048], P('sp', 'tp'), may hold values from -6 to 6
- routes: int32 [1024, 2], P('sp'), may hold values from 0 to 7, all different within a row; in each aligned block of 128 rows (0 to 127, 128 to 255, ...) at most 64 rows name the same one
- route_weight: float32 [1024, 2], P('sp'), may hold values from 0.1 to 1
- w_gate: bfloat16 [8, 2816, 2048], P('sp', 'tp'), may hold values from -0.125 to 0.125
- w_up: bfloat16 [8, 2816, 2048], P('sp', 'tp'), may hold values from -0.125 to 0.125
- w_down: bfloat16 [8, 2816, 2048], P('sp', 'tp'), may hold values from -0.109375 to 0.109375
- v_value: bfloat16 [1024, 1024], P('sp', 'tp'), may hold values from -6 to 6
- v_gate: bfloat16 [1024, 1024], P('sp', 'tp'), may hold values from -12 to 12
- conv_out: bfloat16 [1024, 1024], P('sp', 'tp'), may hold values from -6 to 6
- row_mean: float32 [1024], P('sp'), may hold values from -3 to 3
- row_rstd: float32 [1024], P('sp'), may hold values from 0.5 to 2
- ln_gain: float32 [1024], P('tp'), may hold values from 0.1 to 1.9
- taps: bfloat16 [31, 1024], P(None, 'tp'), may hold values from -1 to 1
- out_proj: bfloat16 [2048, 1024], P('sp', 'tp'), may hold values from -0.1875 to 0.1875
Outputs:
- gate_grad: bfloat16 [8, 2816, 2048], P('sp', 'tp')
- up_grad: bfloat16 [8, 2816, 2048], P('sp', 'tp')
- down_grad: bfloat16 [8, 2816, 2048], P('sp', 'tp')
- proj_grad: float32 [2048, 1024], P('sp', 'tp')
- stream_grad: bfloat16 [1024, 2048], P('sp', 'tp')
- value_grad: bfloat16 [1024, 1024], P('sp', 'tp')
- gating_grad: bfloat16 [1024, 1024], P('sp', 'tp')
Inputs may be any that keep to these rules, and one draw needn't show every extreme that they name: `routes`: in the rows of one device no expert is named more than 64 times.
All inputs are finite; a program needn't handle non-finite values.
Results may differ from a plain program's by a relative error of at most 0.025.
Values may be sent and summed in bfloat16 or wider, within the bound.
A program may use at most 64 MiB of HBM per device.

v0:
```python
import functools

import jax
import jax.numpy as jnp
from jax import lax
from jax.experimental import pallas as pl
from jax.experimental.pallas import tpu as pltpu
from jax.sharding import PartitionSpec as P


def passed_along(value, axis, steps):
    count = lax.axis_size(axis)
    leading, last = (max(0, -steps), min(count, count - steps))
    return lax.ppermute(value, axis, [(source, source + steps) for source in range(leading, last)])


def route_targets(routes, experts, capacity):
    flat_routes = routes.reshape(-1)
    member = (flat_routes[:, None] == jnp.arange(experts, dtype=jnp.int32)[None, :]).astype(
        jnp.int32
    )
    earlier = jnp.cumsum(member, axis=0) - member
    slot_index = jnp.sum(earlier * member, axis=1)
    return flat_routes * capacity + slot_index


def contract_rows(left, right):
    return lax.dot_general(
        left, right, (((0,), (0,)), ((), ())), preferred_element_type=jnp.float32
    )


def contract_cols(left, right):
    return lax.dot_general(
        left, right, (((1,), (1,)), ((), ())), preferred_element_type=jnp.float32
    )


def plain_shards(
    moe_input,
    cotangent,
    routes,
    route_weight,
    w_gate,
    w_up,
    w_down,
    v_value,
    v_gate,
    conv_out,
    row_mean,
    row_rstd,
    ln_gain,
    taps,
    out_proj,
):
    experts = lax.axis_size("sp")
    tokens = routes.shape[0]
    capacity = 4 * tokens // experts
    total = experts * capacity
    buffer_row = route_targets(routes, experts, capacity)
    token_index = jnp.arange(2 * tokens, dtype=jnp.int32) // 2
    weights = route_weight.reshape(-1)
    width = moe_input.shape[1]
    picked = moe_input[token_index]
    weighted = (weights[:, None] * cotangent[token_index].astype(jnp.float32)).astype(jnp.bfloat16)
    rows_buf = jnp.zeros((total, width), jnp.bfloat16).at[buffer_row].set(picked)
    cotan_buf = jnp.zeros((total, width), jnp.bfloat16).at[buffer_row].set(weighted)
    rows_buf, cotan_buf = (
        rows_buf.reshape(experts, capacity, width),
        cotan_buf.reshape(experts, capacity, width),
    )
    part_rows, part_cotan = (
        lax.all_to_all(rows_buf, "sp", split_axis=0, concat_axis=0, tiled=True),
        lax.all_to_all(cotan_buf, "sp", split_axis=0, concat_axis=0, tiled=True),
    )
    arrived_rows, arrived_cotan = (
        lax.all_gather(part_rows, "tp", axis=2, tiled=True),
        lax.all_gather(part_cotan, "tp", axis=2, tiled=True),
    )
    width = arrived_rows.shape[2]
    expert_in = arrived_rows.reshape(total, width)
    expert_cot = arrived_cotan.reshape(total, width)
    gate_w = w_gate[0]
    up_w = w_up[0]
    down_w = w_down[0]
    gate_pre = contract_cols(expert_in, gate_w)
    up_pre = contract_cols(expert_in, up_w)
    gate_sig = jax.nn.sigmoid(gate_pre)
    gate_act = gate_pre * gate_sig
    hidden = (gate_act * up_pre).astype(jnp.bfloat16)
    down_g = contract_rows(hidden, expert_cot).astype(jnp.bfloat16)
    hidden_grad = contract_cols(expert_cot, down_w)
    gate_delta = (hidden_grad * up_pre * gate_sig * (1.0 + gate_pre * (1.0 - gate_sig))).astype(
        jnp.bfloat16
    )
    up_delta = (hidden_grad * gate_act).astype(jnp.bfloat16)
    gate_g = contract_rows(gate_delta, expert_in).astype(jnp.bfloat16)
    up_g = contract_rows(up_delta, expert_in).astype(jnp.bfloat16)
    partial_value = jnp.dot(gate_delta, gate_w, preferred_element_type=jnp.float32) + jnp.dot(
        up_delta, up_w, preferred_element_type=jnp.float32
    )
    row_share = lax.psum_scatter(
        partial_value.astype(jnp.bfloat16), "tp", scatter_dimension=1, tiled=True
    )
    slice_width = row_share.shape[1]
    returned = lax.all_to_all(
        row_share.reshape(experts, capacity, slice_width),
        "sp",
        split_axis=0,
        concat_axis=0,
        tiled=True,
    )
    mine = (
        returned.reshape(total, slice_width)[buffer_row]
        .astype(jnp.float32)
        .reshape(tokens, 2, slice_width)
    )
    stream = (cotangent.astype(jnp.float32) + (mine[:, 0] + mine[:, 1])).astype(jnp.bfloat16)
    full_stream = lax.all_gather(stream, "tp", axis=1, tiled=True)
    normed = (conv_out.astype(jnp.float32) - row_mean[:, None]) * row_rstd[:, None]
    scaled_norm = normed * ln_gain[None, :]
    norm_sig = jax.nn.sigmoid(scaled_norm)
    mixed = (scaled_norm * norm_sig).astype(jnp.bfloat16)
    columns = full_stream
    mixed_grad = jnp.dot(
        columns,
        lax.all_gather(out_proj, "sp", axis=0, tiled=True),
        preferred_element_type=jnp.float32,
    )
    columns = full_stream
    proj_g = lax.psum_scatter(
        contract_rows(columns, mixed).astype(jnp.bfloat16), "sp", scatter_dimension=0, tiled=True
    ).astype(jnp.float32)
    channels = out_proj.shape[1] * lax.axis_size("tp")
    norm_grad = mixed_grad * norm_sig * (1.0 + scaled_norm * (1.0 - norm_sig)) * ln_gain[None, :]
    first_sum, second_sum = lax.psum(
        (jnp.sum(norm_grad, axis=1), jnp.sum(norm_grad * normed, axis=1)), "tp"
    )
    first_mean = first_sum[:, None] / channels
    second_mean = second_sum[:, None] / channels
    conv_grad = row_rstd[:, None] * (norm_grad - first_mean - normed * second_mean)
    kernel = taps.shape[0]
    following = passed_along(conv_grad[: kernel - 1], "sp", -1)
    extended = jnp.concatenate([conv_grad, following], axis=0)
    tap_values = taps.astype(jnp.float32)
    unit_grad = jnp.zeros_like(conv_grad)
    for offset in range(kernel):
        lead = kernel - 1 - offset
        unit_grad = unit_grad + tap_values[offset][None, :] * extended[lead : lead + tokens]
    value_sig = jax.nn.sigmoid(v_gate.astype(jnp.float32))
    value_g = (unit_grad * value_sig).astype(jnp.bfloat16)
    gating_g = (unit_grad * v_value.astype(jnp.float32) * value_sig * (1.0 - value_sig)).astype(
        jnp.bfloat16
    )
    return (gate_g[None], up_g[None], down_g[None], proj_g, stream, value_g, gating_g)


VMEM = pl.BlockSpec(memory_space=pltpu.VMEM)


def remote(src, dst, send_sem, recv_sem, sp, tp):
    return pltpu.make_async_remote_copy(
        src_ref=src,
        dst_ref=dst,
        send_sem=send_sem,
        recv_sem=recv_sem,
        device_id={"sp": sp, "tp": tp},
        device_id_type=pl.DeviceIdType.MESH,
    )


def greet(peers):
    barrier = pltpu.get_barrier_semaphore()
    for sp, tp in peers:
        pl.semaphore_signal(
            barrier, inc=1, device_id={"sp": sp, "tp": tp}, device_id_type=pl.DeviceIdType.MESH
        )
    pl.semaphore_wait(barrier, len(peers))


def rows_of(ref, index, count):
    return ref.at[pl.ds(pl.multiple_of(index * count, count), count)]


class ChipGather:
    def __init__(self, own, everyone, sems, me, tp, count):
        self.own, self.everyone, self.me, self.tp, self.count = own, everyone, me, tp, count
        self.send, self.recv, self.relay, self.local = sems
        self.partner = me + 1 - 2 * (me % 2)
        self.ahead = [(me + 2 * e) % count for e in range(1, count // 2)]
        self.behind = [(me + count - 2 * e) % count for e in range(1, count // 2)]

    def block(self, index):
        return rows_of(self.everyone, index, self.own.shape[0])

    def first(self, target):
        return remote(
            self.own,
            self.block(self.me),
            self.send.at[target],
            self.recv.at[self.me],
            target,
            self.tp,
        )

    def onward(self, origin):
        return remote(
            self.block(origin),
            self.block(origin),
            self.relay.at[origin],
            self.recv.at[origin],
            self.partner,
            self.tp,
        )

    def start(self):
        pltpu.make_async_copy(self.own, self.block(self.me), self.local).start()
        for target in self.ahead + [self.partner]:
            self.first(target).start()

    def pass_on(self):
        for origin in self.behind:
            self.onward(origin).wait_recv()
            self.onward(origin).start()

    def finish(self):
        pltpu.make_async_copy(self.own, self.block(self.me), self.local).wait()
        for step in range(self.count // 2):
            origin = (self.partner + 2 * step) % self.count
            self.onward(origin).wait_recv()
        for target in self.ahead + [self.partner]:
            self.first(target).wait_send()
        for origin in self.behind:
            self.onward(origin).wait_send()


def gather_sems(count):
    return [
        pltpu.SemaphoreType.DMA((count,)),
        pltpu.SemaphoreType.DMA((count,)),
        pltpu.SemaphoreType.DMA((count,)),
        pltpu.SemaphoreType.DMA,
    ]


def dispatch_kernel(
    count, rows, cot, mixed, rows_out, cot_out, mixed_out, send, recv, local, *mixed_sems
):
    me, tp = lax.axis_index("sp"), lax.axis_index("tp")
    capacity, width = rows.shape[1:]
    across, down, corner = tp + 1 - 2 * (tp % 2), (tp + 2) % 4, 3 - tp
    others = [(me + d) % count for d in range(1, count)]
    greet([(other, tp) for other in others] + [(me, across), (me, down)])
    arrays = ((rows, rows_out), (cot, cot_out))

    def block(a, source, owner):
        return arrays[a][1].at[
            pl.ds(pl.multiple_of(source * capacity, capacity), capacity),
            pl.ds(pl.multiple_of(owner * width, 128), width),
        ]

    def own_copy(a):
        return pltpu.make_async_copy(arrays[a][0].at[me], block(a, me, tp), local.at[a])

    def out_copy(a, target):
        return remote(
            arrays[a][0].at[target],
            block(a, me, tp),
            send.at[a, target, 0],
            recv.at[a, me, tp],
            target,
            tp,
        )

    def side_copy(a, source, owner, target, lane):
        spot = block(a, source, owner)
        return remote(spot, spot, send.at[a, source, lane], recv.at[a, source, owner], me, target)

    for a in range(2):
        own_copy(a).start()
    for target in others:
        for a in range(2):
            out_copy(a, target).start()
    gather = ChipGather(mixed, mixed_out, mixed_sems, me, tp, count)
    gather.start()

    def relay_of(step):
        return (across, down) if step % 2 == 0 else (down, across)

    def relay(step):
        source = (me + count - step) % count
        owner, target = relay_of(step)
        for a in range(2):
            side_copy(a, source, owner, target, 3).wait_recv()
            side_copy(a, source, owner, target, 3).start()

    for step in range(count):
        source = (me + count - step) % count
        for a in range(2):
            if step == 0:
                own_copy(a).wait()
            else:
                side_copy(a, source, tp, across, 1).wait_recv()
            side_copy(a, source, tp, across, 1).start()
            side_copy(a, source, tp, down, 2).start()
        if step >= 1:
            relay(step - 1)
    relay(count - 1)
    gather.pass_on()
    for step in range(count):
        source = (me + count - step) % count
        owner, target = relay_of(step)
        for a in range(2):
            side_copy(a, source, target, across, 1).wait_recv()
            side_copy(a, source, corner, across, 1).wait_recv()
            side_copy(a, source, tp, across, 1).wait_send()
            side_copy(a, source, tp, down, 2).wait_send()
            side_copy(a, source, owner, target, 3).wait_send()
    for target in others:
        for a in range(2):
            out_copy(a, target).wait_send()
    gather.finish()


def dispatch(rows, cot, mixed, count):
    capacity, width = rows.shape[1:]
    full = jax.ShapeDtypeStruct((count * capacity, width * lax.axis_size("tp")), jnp.bfloat16)
    return pl.pallas_call(
        functools.partial(dispatch_kernel, count),
        out_shape=(
            full,
            full,
            jax.ShapeDtypeStruct((count * mixed.shape[0], mixed.shape[1]), mixed.dtype),
        ),
        in_specs=[VMEM] * 3,
        out_specs=(VMEM,) * 3,
        scratch_shapes=[
            pltpu.SemaphoreType.DMA((2, count, 4)),
            pltpu.SemaphoreType.DMA((2, count, 4)),
            pltpu.SemaphoreType.DMA((2,)),
        ]
        + gather_sems(count),
        compiler_params=pltpu.CompilerParams(
            collective_id=0, has_side_effects=True, vmem_limit_bytes=40 << 20
        ),
        name="dispatch",
        cost_estimate=pl.CostEstimate(
            flops=0, bytes_accessed=200 * rows.size * 2, transcendentals=0
        ),
    )(rows, cot, mixed)


def combine_kernel(
    count,
    partial_ref,
    cot,
    pick,
    proj,
    hidden,
    gate_delta,
    up_delta,
    expert_in,
    expert_cot,
    stream,
    proj_out,
    grads,
    landed,
    middle,
    reduced,
    back,
    send,
    recv,
    back_send,
    back_recv,
    wide_send,
    wide_recv,
    *proj_sems,
):
    me, tp = lax.axis_index("sp"), lax.axis_index("tp")
    capacity, width = reduced.shape[1:]
    units = hidden.shape[0]
    across, down, corner = tp + 1 - 2 * (tp % 2), (tp + 2) % 4, 3 - tp
    group = (across, down, corner)
    others = [(me + d) % count for d in range(1, count)]
    greet([(other, tp) for other in others] + [(me, other) for other in group])

    def share(source, owner):
        return partial_ref.at[
            pl.ds(pl.multiple_of(source * capacity, capacity), capacity),
            pl.ds(pl.multiple_of(owner * width, 128), width),
        ]

    order = others + [me]

    def sides(step):
        return (across, down) if step % 2 == 0 else (down, across)

    def share_copy(step, q):
        source, near = order[step], sides(step)[0]
        return remote(
            share(source, corner if q == 1 else near),
            landed.at[q, source],
            send.at[source, q],
            recv.at[source, q],
            me,
            near,
        )

    def middle_copy(step):
        source = order[step]
        return remote(
            middle.at[source],
            landed.at[2, source],
            send.at[source, 2],
            recv.at[source, 2],
            me,
            sides(step)[1],
        )

    def back_copy(target):
        return remote(
            reduced.at[target],
            rows_of(back, me, capacity),
            back_send.at[target],
            back_recv.at[me],
            target,
            tp,
        )

    def begin(step):
        for q in (1, 0):
            share_copy(step, q).start()

    def forward(step):
        source = order[step]
        share_copy(step, 1).wait_recv()
        own = share(source, sides(step)[1])[...].astype(jnp.float32)
        middle[source] = (own + landed[1, source].astype(jnp.float32)).astype(jnp.bfloat16)
        middle_copy(step).start()

    def settle(step):
        source = order[step]
        share_copy(step, 0).wait_recv()
        middle_copy(step).wait_recv()
        total = share(source, tp)[...].astype(jnp.float32)
        total = total + landed[0, source].astype(jnp.float32)
        total = (total + landed[2, source].astype(jnp.float32)).astype(jnp.bfloat16)
        if step < count - 1:
            reduced[source] = total
            back_copy(source).start()
        else:
            back[pl.ds(pl.multiple_of(me * capacity, capacity), capacity), :] = total

    pieces = 4 if units % 64 == 0 else 1
    tile = units // pieces
    spots = pieces * 4
    products = ((gate_delta, expert_in), (up_delta, expert_in), (hidden, expert_cot))

    def product(spot, carry):
        rows = pl.ds(pl.multiple_of(spot // 4 * tile, 16), tile)
        columns = pl.ds(pl.multiple_of(spot % 4 * width, 128), width)
        for a, (left, right) in enumerate(products):
            value = jnp.dot(
                left[rows, :], right[:, columns], preferred_element_type=jnp.float32
            )
            grads[a, rows, columns] = value.astype(jnp.bfloat16)
        return carry

    window = min(3, count)
    for step in range(window):
        begin(step)
    gather = ChipGather(proj, proj_out, proj_sems, me, tp, count)
    gather.start()
    for step in range(count):
        lax.fori_loop(spots * step // count, spots * (step + 1) // count, product, 0)
        if step + window < count:
            begin(step + window)
        forward(step)
        if step >= 1:
            settle(step - 1)
    settle(count - 1)
    gather.pass_on()
    for other in others:
        remote(
            reduced.at[other],
            rows_of(back, other, capacity),
            back_send.at[other],
            back_recv.at[other],
            other,
            tp,
        ).wait_recv()
    mine = jnp.dot(pick[...], back[...], preferred_element_type=jnp.float32)
    columns = pl.ds(pl.multiple_of(tp * width, 128), width)
    stream[:, columns] = (cot[...].astype(jnp.float32) + mine).astype(jnp.bfloat16)

    def wide_copy(q):
        spot = stream.at[:, columns]
        return remote(spot, spot, wide_send.at[q], wide_recv.at[q], me, group[q])

    for q in range(3):
        wide_copy(q).start()
    for q in range(3):
        wide_copy(q).wait()
    for step in range(count):
        share_copy(step, 0).wait_send()
        share_copy(step, 1).wait_send()
        middle_copy(step).wait_send()
    for other in others:
        back_copy(other).wait_send()
    gather.finish()


def combine(partial_value, cot, pick, proj, hidden, gate_delta, up_delta, rows, rows_cot, count):
    tokens, width = cot.shape
    capacity = partial_value.shape[0] // count
    return pl.pallas_call(
        functools.partial(combine_kernel, count),
        out_shape=(
            jax.ShapeDtypeStruct((tokens, partial_value.shape[1]), jnp.bfloat16),
            jax.ShapeDtypeStruct((count * proj.shape[0], proj.shape[1]), jnp.bfloat16),
            jax.ShapeDtypeStruct((3, hidden.shape[0], partial_value.shape[1]), jnp.bfloat16),
        ),
        in_specs=[VMEM] * 9,
        out_specs=(VMEM,) * 3,
        scratch_shapes=[
            pltpu.VMEM((3, count, capacity, width), jnp.bfloat16),
            pltpu.VMEM((count, capacity, width), jnp.bfloat16),
            pltpu.VMEM((count, capacity, width), jnp.bfloat16),
            pltpu.VMEM((count * capacity, width), jnp.bfloat16),
            pltpu.SemaphoreType.DMA((count, 3)),
            pltpu.SemaphoreType.DMA((count, 3)),
            pltpu.SemaphoreType.DMA((count,)),
            pltpu.SemaphoreType.DMA((count,)),
            pltpu.SemaphoreType.DMA((3,)),
            pltpu.SemaphoreType.DMA((3,)),
        ]
        + gather_sems(count),
        compiler_params=pltpu.CompilerParams(
            collective_id=1, has_side_effects=True, vmem_limit_bytes=40 << 20
        ),
        name="combine",
        cost_estimate=pl.CostEstimate(
            flops=6 * hidden.size * partial_value.shape[1],
            bytes_accessed=50 * partial_value.size * 2,
            transcendentals=0,
        ),
    )(partial_value, cot, pick, proj, hidden, gate_delta, up_delta, rows, rows_cot)


def module_kernel(
    count,
    stream,
    proj,
    mixed,
    conv_out,
    row_mean,
    row_rstd,
    gain,
    taps,
    v_value,
    v_gate,
    proj_grad,
    value_grad,
    gating_grad,
    columns,
    sums,
    arrived,
    extended,
    send,
    recv,
    local,
    sum_send,
    sum_recv,
    edge_send,
    edge_recv,
):
    me, tp = lax.axis_index("sp"), lax.axis_index("tp")
    tokens, channels = conv_out.shape
    depth = stream.shape[1] // count
    halo = extended.shape[0] - tokens
    group = (tp + 1 - 2 * (tp % 2), (tp + 2) % 4, 3 - tp)
    others = [(me + d) % count for d in range(1, count)]
    greet([(other, tp) for other in others] + [(me, other) for other in group])

    def strip(index):
        return stream.at[:, pl.ds(pl.multiple_of(index * depth, 128), depth)]

    def strip_copy(target):
        return remote(
            strip(target),
            rows_of(columns, me, tokens),
            send.at[target],
            recv.at[me],
            target,
            tp,
        )

    own = pltpu.make_async_copy(strip(me), rows_of(columns, me, tokens), local)
    own.start()
    for other in others:
        strip_copy(other).start()
    mixed_grad = jnp.dot(stream[...], proj[...], preferred_element_type=jnp.float32)
    rstd = jnp.broadcast_to(row_rstd[...], (tokens, tokens)).T[:, 0:1]
    mean = jnp.broadcast_to(row_mean[...], (tokens, tokens)).T[:, 0:1]
    normed = (conv_out[...].astype(jnp.float32) - mean) * rstd
    scaled = normed * gain[...]
    sig = jax.nn.sigmoid(scaled)
    norm_grad = mixed_grad * sig * (1.0 + scaled * (1.0 - sig)) * gain[...]
    first = jnp.sum(norm_grad, axis=1, keepdims=True)
    second = jnp.sum(norm_grad * normed, axis=1, keepdims=True)
    lanes = lax.broadcasted_iota(jnp.int32, (tokens, 128), 1)
    pair = jnp.where(lanes % 2 == 0, first, second)
    sums[...] = pair.T[:8]

    def sum_copy(q):
        return remote(sums, arrived.at[q], sum_send.at[q], sum_recv.at[q], me, group[q])

    for q in range(3):
        sum_copy(q).start()
    value_sig = jax.nn.sigmoid(v_gate[...].astype(jnp.float32))
    gating_scale = v_value[...].astype(jnp.float32) * value_sig * (1.0 - value_sig)
    for q in range(3):
        sum_copy(q).wait()
    total = sums[...] + arrived[0] + arrived[1] + arrived[2]
    total = total * (1.0 / (channels * 4))
    means = jnp.concatenate([total] * 16, axis=0).T
    conv_grad = rstd * (norm_grad - means[:, 0:1] - normed * means[:, 1:2])
    extended[:tokens] = conv_grad
    edge = remote(
        extended.at[pl.ds(0, halo)],
        extended.at[pl.ds(tokens, halo)],
        edge_send,
        edge_recv,
        (me + count - 1) % count,
        tp,
    )

    @pl.when(me > 0)
    def _():
        edge.start()

    @pl.when(me == count - 1)
    def _():
        extended[tokens:] = jnp.zeros((halo, channels), jnp.float32)

    @pl.when(me < count - 1)
    def _():
        edge.wait_recv()

    kernel = taps.shape[0]
    unit_grad = jnp.zeros((tokens, channels), jnp.float32)
    for offset in range(kernel):
        lead = kernel - 1 - offset
        tap = taps[offset : offset + 1, :].astype(jnp.float32)
        unit_grad = unit_grad + tap * extended[lead : lead + tokens, :]
    value_grad[...] = (unit_grad * value_sig).astype(jnp.bfloat16)
    gating_grad[...] = (unit_grad * gating_scale).astype(jnp.bfloat16)
    own.wait()
    for other in others:
        remote(
            strip(other),
            rows_of(columns, other, tokens),
            send.at[other],
            recv.at[other],
            other,
            tp,
        ).wait_recv()
    proj_grad[...] = contract_rows(columns[...], mixed[...])
    for other in others:
        strip_copy(other).wait_send()

    @pl.when(me > 0)
    def _():
        edge.wait_send()


def module(stream, proj, mixed, conv_out, row_mean, row_rstd, gain, taps, v_value, v_gate, count):
    tokens, channels = conv_out.shape
    depth = stream.shape[1] // count
    halo = -(-(taps.shape[0] - 1) // 8) * 8
    return pl.pallas_call(
        functools.partial(module_kernel, count),
        out_shape=(
            jax.ShapeDtypeStruct((depth, channels), jnp.float32),
            jax.ShapeDtypeStruct((tokens, channels), jnp.bfloat16),
            jax.ShapeDtypeStruct((tokens, channels), jnp.bfloat16),
        ),
        in_specs=[VMEM] * 10,
        out_specs=(VMEM,) * 3,
        scratch_shapes=[
            pltpu.VMEM((count * tokens, depth), jnp.bfloat16),
            pltpu.VMEM((8, tokens), jnp.float32),
            pltpu.VMEM((3, 8, tokens), jnp.float32),
            pltpu.VMEM((tokens + halo, channels), jnp.float32),
            pltpu.SemaphoreType.DMA((count,)),
            pltpu.SemaphoreType.DMA((count,)),
            pltpu.SemaphoreType.DMA,
            pltpu.SemaphoreType.DMA((3,)),
            pltpu.SemaphoreType.DMA((3,)),
            pltpu.SemaphoreType.DMA,
            pltpu.SemaphoreType.DMA,
        ],
        compiler_params=pltpu.CompilerParams(
            collective_id=2, has_side_effects=True, vmem_limit_bytes=40 << 20
        ),
        name="module",
    )(stream, proj, mixed, conv_out, row_mean, row_rstd, gain, taps, v_value, v_gate)


def kernel_shards(
    moe_input,
    cotangent,
    routes,
    route_weight,
    w_gate,
    w_up,
    w_down,
    v_value,
    v_gate,
    conv_out,
    row_mean,
    row_rstd,
    ln_gain,
    taps,
    out_proj,
):
    experts = lax.axis_size("sp")
    tokens, width = moe_input.shape
    capacity = 4 * tokens // experts
    total = experts * capacity
    flat_routes = routes.reshape(-1)
    member = (flat_routes[:, None] == jnp.arange(experts, dtype=jnp.int32)[None, :]).astype(
        jnp.bfloat16
    )
    index = jnp.arange(2 * tokens, dtype=jnp.int32)
    before = (index[None, :] < index[:, None]).astype(jnp.bfloat16)
    earlier = jnp.dot(before, member, preferred_element_type=jnp.float32)
    slot_index = jnp.sum(earlier * member.astype(jnp.float32), axis=1).astype(jnp.int32)
    buffer_row = (flat_routes * capacity + slot_index).reshape(tokens, 2)
    places = jnp.arange(total, dtype=jnp.int32)
    place0 = (buffer_row[:, 0][:, None] == places[None, :]).astype(jnp.bfloat16)
    place1 = (buffer_row[:, 1][:, None] == places[None, :]).astype(jnp.bfloat16)
    pick = place0 + place1
    cot32 = cotangent.astype(jnp.float32)
    weighted = jnp.concatenate(
        [
            (route_weight[:, 0:1] * cot32).astype(jnp.bfloat16),
            (route_weight[:, 1:2] * cot32).astype(jnp.bfloat16),
        ],
        axis=0,
    )
    rows_buf = contract_rows(pick, moe_input).astype(jnp.bfloat16)
    cot_buf = contract_rows(jnp.concatenate([place0, place1], axis=0), weighted).astype(
        jnp.bfloat16
    )
    normed = (conv_out.astype(jnp.float32) - row_mean[:, None]) * row_rstd[:, None]
    scaled_norm = normed * ln_gain[None, :]
    mixed = (scaled_norm * jax.nn.sigmoid(scaled_norm)).astype(jnp.bfloat16)
    expert_in, expert_cot, mixed_all = dispatch(
        rows_buf.reshape(experts, capacity, width),
        cot_buf.reshape(experts, capacity, width),
        mixed,
        experts,
    )
    gate_w = w_gate[0]
    up_w = w_up[0]
    down_w = w_down[0]
    gate_pre = contract_cols(gate_w, expert_in)
    up_pre = contract_cols(up_w, expert_in)
    gate_sig = jax.nn.sigmoid(gate_pre)
    gate_act = gate_pre * gate_sig
    hidden = (gate_act * up_pre).astype(jnp.bfloat16)
    hidden_grad = contract_cols(down_w, expert_cot)
    gate_delta = (hidden_grad * up_pre * gate_sig * (1.0 + gate_pre * (1.0 - gate_sig))).astype(
        jnp.bfloat16
    )
    up_delta = (hidden_grad * gate_act).astype(jnp.bfloat16)
    partial_value = contract_rows(gate_delta, gate_w) + contract_rows(up_delta, up_w)
    stream_full, proj_full, grads = combine(
        partial_value.astype(jnp.bfloat16),
        cotangent,
        pick,
        out_proj,
        hidden,
        gate_delta,
        up_delta,
        expert_in,
        expert_cot,
        experts,
    )
    proj_g, value_g, gating_g = module(
        stream_full,
        proj_full,
        mixed_all,
        conv_out,
        row_mean[None, :],
        row_rstd[None, :],
        ln_gain[None, :],
        taps,
        v_value,
        v_gate,
        experts,
    )
    stream = lax.dynamic_slice_in_dim(stream_full, lax.axis_index("tp") * width, width, 1)
    return (grads[0:1], grads[1:2], grads[2:3], proj_g, stream, value_g, gating_g)


def shards(*blocks):
    tokens, width = blocks[0].shape
    depth, channels = blocks[-1].shape
    experts = lax.axis_size("sp")
    square = lax.axis_size("tp") == 4 and experts % 2 == 0 and tokens == 128
    capacity = 4 * tokens // experts
    tiled = width % 128 == 0 and depth % 128 == 0 and channels % 128 == 0 and capacity % 16 == 0
    if square and tiled:
        return kernel_shards(*blocks)
    return plain_shards(*blocks)


def solution(mesh):
    return jax.shard_map(
        shards,
        mesh=mesh,
        in_specs=(
            P("sp", "tp"),
            P("sp", "tp"),
            P("sp", None),
            P("sp", None),
            P("sp", "tp", None),
            P("sp", "tp", None),
            P("sp", "tp", None),
            P("sp", "tp"),
            P("sp", "tp"),
            P("sp", "tp"),
            P("sp"),
            P("sp"),
            P("tp"),
            P(None, "tp"),
            P("sp", "tp"),
        ),
        out_specs=(
            P("sp", "tp", None),
            P("sp", "tp", None),
            P("sp", "tp", None),
            P("sp", "tp"),
            P("sp", "tp"),
            P("sp", "tp"),
            P("sp", "tp"),
        ),
        check_vma=False,
    )
```

profile of v0, /device:TPU:9, one launch (start us, length us, event | category | flops | bytes accessed | tf_op | source)
XLA Modules:
  0.0 134.8 jit_solution(9573087688970722427)
XLA Ops:
  0.6 0.0 copy-start
  0.6 0.0 copy-start.13
  0.7 0.0 copy-start.2
  0.7 0.0 copy-start.10
  0.7 0.0 copy-start.9
  0.7 0.9 copy.28
  1.6 0.1 eq.45
  1.8 0.2 fusion.19
  2.0 0.1 convert_element_type.56
  2.1 0.1 copy.29
  2.2 0.9 multiply_add_fusion
  3.1 0.1 fusion.28
  3.2 0.8 slice_bitcast_fusion.1
  3.9 1.0 fusion.20
  5.0 0.3 convolution_convert_fusion
  5.3 0.0 copy-done.13
  5.3 0.4 convolution_convert_fusion.1
  5.7 0.0 copy-done.2
  5.7 0.0 copy-done.10
  5.7 0.0 copy-done.9
  5.7 0.0 copy-done.8
  5.7 0.1 multiply_convert_fusion.3.mixed
  5.9 41.6 %dispatch.1 = (bf16[512,2048]{1,0:T(8,128)(2,1)S(1)}, bf16[512,2048]{1,0:T(8,128)(2,1)S(1)}, bf16[1024,256]{1,0:T(8,128)(2,1)S(1)}) custom-call(bf16[8,64,512]{2,1,0:T(8,128)(2,1)S(1)} %bitcast.46, bf16[8,64,512]{2,1,0:T(8,128)(2,1)S(1)} %bitcast.47, bf16[128,256]{1,0:T(8,128)(2,1)S(1)} %multiply_convert_fusion.3.mixed), custom_call_target="tpu_custom_call" | custom-call | bytes 104857600 | tf_op jit(solution)/shard_map/dispatch/pallas_call | solution.py:328
  47.5 0.0 copy-start.14
  47.5 1.7 %fusion.15 = f32[704,512]{1,0:T(8,128)S(1)} fusion(bf16[512,2048]{1,0:T(8,128)(2,1)S(1)} %get-tuple-element.17.expert_in, bf16[1,704,2048]{2,1,0:T(8,128)(2,1)S(1)} %copy-done.12), kind=kOutput, calls=%fused_computation.12 | convolution fusion | flops 1476395008 | bytes 6422528 | tf_op jit(solution)/shard_map/dot_general | solution.py:34
  49.2 0.1 copy-done.14
  49.3 1.7 %fusion.9 = f32[704,512]{1,0:T(8,128)S(1)} fusion(bf16[512,2048]{1,0:T(8,128)(2,1)S(1)} %get-tuple-element.16.expert_cot, bf16[1,704,2048]{2,1,0:T(8,128)(2,1)S(1)} %copy-done.14), kind=kOutput, calls=%fused_computation.10 | convolution fusion | flops 1476395008 | bytes 6422528 | tf_op jit(solution)/shard_map/dot_general | solution.py:34
  51.0 0.0 copy-done
  51.0 2.2 %multiply_convert_fusion = (bf16[704,512]{1,0:T(8,128)(2,1)S(1)}, bf16[704,512]{1,0:T(8,128)(2,1)S(1)}, bf16[704,512]{1,0:T(8,128)(2,1)S(1)}) fusion(f32[704,512]{1,0:T(8,128)S(1)} %fusion.15, f32[704,512]{1,0:T(8,128)S(1)} %fusion.9, bf16[512,2048]{1,0:T(8,128)(2,1)S(1)} %get-tuple-element.17.expert_in, bf16[1,704,2048]{2,1,0:T(8,128)(2,1)S(1)} %copy-done), kind=kOutput, calls=%fused_computation.13 | convolution fusion | flops 1481801728 | bytes 10027008 | tf_op jit(solution)/shard_map/dot_general | solution.py:34
  53.3 1.8 %fusion = f32[512,2048]{1,0:T(8,128)S(1)} fusion(bf16[704,512]{1,0:T(8,128)(2,1)S(1)} %get-tuple-element.29.gate_delta, bf16[1,704,2048]{2,1,0:T(8,128)(2,1)S(1)} %copy-done.12), kind=kOutput, calls=%fused_computation.1 | convolution fusion | flops 1476395008 | bytes 7798784 | tf_op jit(solution)/shard_map/dot_general | solution.py:28
  55.1 0.0 copy-start.3
  55.1 0.0 copy-start.11
  55.1 1.8 %add_convert_fusion.partial_ref = bf16[512,2048]{1,0:T(8,128)(2,1)S(1)} fusion(f32[512,2048]{1,0:T(8,128)S(1)} %fusion, bf16[704,512]{1,0:T(8,128)(2,1)S(1)} %get-tuple-element.30.up_delta, bf16[1,704,2048]{2,1,0:T(8,128)(2,1)S(1)} %copy-done), kind=kOutput, calls=%fused_computation | convolution fusion | flops 1478492160 | bytes 9895936 | tf_op jit(solution)/shard_map/dot_general | solution.py:28
  57.0 0.1 fusion.30.pick
  57.1 0.0 copy-done.3
  57.1 0.0 copy-done.11
  57.1 0.0 copy-start.5
  57.1 0.0 copy-start.6
  57.1 0.0 copy-start.7
  57.1 50.6 %combine.1 = (bf16[128,2048]{1,0:T(8,128)(2,1)S(1)}, bf16[2048,256]{1,0:T(8,128)(2,1)S(1)}, bf16[3,704,2048]{2,1,0:T(8,128)(2,1)}) custom-call(bf16[512,2048]{1,0:T(8,128)(2,1)S(1)} %add_convert_fusion.partial_ref, bf16[128,512]{1,0:T(8,128)(2,1)S(1)} %copy-done.3, bf16[128,512]{1,0:T(8,128)(2,1)S(1)} %fusion.30.pick, bf16[256,256]{1,0:T(8,128)(2,1)S(1)} %copy-done.11, ...), custom_call_target="tpu_custom_call" | custom-call | flops 4429185024 | bytes 104857600 | tf_op jit(solution)/shard_map/combine/pallas_call | solution.py:516
  107.8 16.4 %module.1 = (f32[256,256]{1,0:T(8,128)S(1)}, bf16[128,256]{1,0:T(8,128)(2,1)S(1)}, bf16[128,256]{1,0:T(8,128)(2,1)S(1)}) custom-call(bf16[128,2048]{1,0:T(8,128)(2,1)S(1)} %get-tuple-element.19.stream, bf16[2048,256]{1,0:T(8,128)(2,1)S(1)} %get-tuple-element.20.proj, bf16[1024,256]{1,0:T(8,128)(2,1)S(1)} %get-tuple-element.21.mixed, ...), custom_call_target="tpu_custom_call" | custom-call | tf_op jit(solution)/shard_map/module/pallas_call | solution.py:681
  124.3 0.0 copy-start.1
  124.3 0.0 copy-start.4
  124.3 6.1 %fusion.35 = (bf16[1,704,2048]{2,1,0:T(8,128)(2,1)}, bf16[1,704,2048]{2,1,0:T(8,128)(2,1)}, bf16[1,704,2048]{2,1,0:T(8,128)(2,1)}) fusion(bf16[3,704,2048]{2,1,0:T(8,128)(2,1)} %get-tuple-element.18), kind=kLoop, calls=%fused_computation.49 | loop fusion | bytes 17301504 | tf_op jit(solution)/shard_map/slice | solution.py:805
  130.4 0.7 constant_dynamic-slice_fusion
  131.0 1.7 %copy.33 = f32[256,256]{1,0:T(8,128)} copy(f32[256,256]{1,0:T(8,128)} %copy-done.1) | data formatting | bytes 524288
  132.7 1.5 %copy.34 = bf16[128,256]{1,0:T(8,128)(2,1)} copy(bf16[128,256]{1,0:T(8,128)(2,1)} %copy-done.4) | data formatting | bytes 131072
  134.2 0.6 copy.35
  (10 shorter events, 0.0 us)
Async XLA Ops:
  0.6 50.4 %copy-start = (bf16[1,704,2048]{2,1,0:T(8,128)(2,1)S(1)}, bf16[1,704,2048]{2,1,0:T(8,128)(2,1)}, u32[]{:S(2)}) copy-start(bf16[1,704,2048]{2,1,0:T(8,128)(2,1)} %param.20) | copy-start | bytes 8650756
  0.6 4.6 %copy-start.13 = (bf16[128,512]{1,0:T(8,128)(2,1)S(1)}, bf16[128,512]{1,0:T(8,128)(2,1)}, u32[]{:S(2)}) copy-start(bf16[128,512]{1,0:T(8,128)(2,1)} %param.15) | copy-start | bytes 393220
  0.7 5.0 %copy-start.2 = (bf16[128,256]{1,0:T(8,128)(2,1)S(1)}, bf16[128,256]{1,0:T(8,128)(2,1)}, u32[]{:S(2)}) copy-start(bf16[128,256]{1,0:T(8,128)(2,1)} %conv_out.1) | copy-start | bytes 196612
  0.7 5.0 %copy-start.10 = (f32[128]{0:T(128)S(1)}, f32[128]{0:T(128)}, u32[]{:S(2)}) copy-start(f32[128]{0:T(128)} %param.25) | copy-start | bytes 1540
  0.7 5.0 %copy-start.9 = (f32[128]{0:T(128)S(1)}, f32[128]{0:T(128)}, u32[]{:S(2)}) copy-start(f32[128]{0:T(128)} %param.26) | copy-start | bytes 1540
  0.7 5.0 %copy-start.8 = (f32[256]{0:T(256)S(1)}, f32[256]{0:T(256)}, u32[]{:S(2)}) copy-start(f32[256]{0:T(256)} %param.27) | copy-start | bytes 3076
  2.2 45.3 %copy-start.12 = (bf16[1,704,2048]{2,1,0:T(8,128)(2,1)S(1)}, bf16[1,704,2048]{2,1,0:T(8,128)(2,1)}, u32[]{:S(2)}) copy-start(bf16[1,704,2048]{2,1,0:T(8,128)(2,1)} %param.19) | copy-start | bytes 8650756
  47.5 1.8 %copy-start.14 = (bf16[1,704,2048]{2,1,0:T(8,128)(2,1)S(1)}, bf16[1,704,2048]{2,1,0:T(8,128)(2,1)}, u32[]{:S(2)}) copy-start(bf16[1,704,2048]{2,1,0:T(8,128)(2,1)} %param.21) | copy-start | bytes 8650756
  55.1 2.0 %copy-start.3 = (bf16[128,512]{1,0:T(8,128)(2,1)S(1)}, bf16[128,512]{1,0:T(8,128)(2,1)}, u32[]{:S(2)}) copy-start(bf16[128,512]{1,0:T(8,128)(2,1)} %cot.1) | copy-start | bytes 393220
  55.1 2.0 %copy-start.11 = (bf16[256,256]{1,0:T(8,128)(2,1)S(1)}, bf16[256,256]{1,0:T(8,128)(2,1)}, u32[]{:S(2)}) copy-start(bf16[256,256]{1,0:T(8,128)(2,1)} %proj.1) | copy-start | bytes 393220
  57.1 50.7 %copy-start.5 = (bf16[128,256]{1,0:T(8,128)(2,1)S(1)}, bf16[128,256]{1,0:T(8,128)(2,1)}, u32[]{:S(2)}) copy-start(bf16[128,256]{1,0:T(8,128)(2,1)} %v_value.1) | copy-start | bytes 196612
  57.1 50.7 %copy-start.6 = (bf16[128,256]{1,0:T(8,128)(2,1)S(1)}, bf16[128,256]{1,0:T(8,128)(2,1)}, u32[]{:S(2)}) copy-start(bf16[128,256]{1,0:T(8,128)(2,1)} %v_gate.1) | copy-start | bytes 196612
  57.1 50.7 %copy-start.7 = (bf16[31,256]{1,0:T(8,128)(2,1)S(1)}, bf16[31,256]{1,0:T(8,128)(2,1)}, u32[]{:S(2)}) copy-start(bf16[31,256]{1,0:T(8,128)(2,1)} %taps.1) | copy-start | bytes 47620
  124.3 6.1 %copy-start.1 = (f32[256,256]{1,0:T(8,128)}, f32[256,256]{1,0:T(8,128)S(1)}, u32[]{:S(2)}) copy-start(f32[256,256]{1,0:T(8,128)S(1)} %get-tuple-element.49) | copy-start | bytes 786436
  124.3 6.1 %copy-start.4 = (bf16[128,256]{1,0:T(8,128)(2,1)}, bf16[128,256]{1,0:T(8,128)(2,1)S(1)}, u32[]{:S(2)}) copy-start(bf16[128,256]{1,0:T(8,128)(2,1)S(1)} %get-tuple-element.51) | copy-start | bytes 196612
where the time goes:
time: 135 us
  Pallas kernels  109 us (81%)
  local copies, waits for them, and re-layouts  12.7 us (9%)
  matrix products  10.2 us (8%)
  other arithmetic  2.22 us (2%)
    pallas_call x1, Pallas kernels, combine(): pl.pallas_call(functools.partial(combine_kernel, count), out_shape=(jax.S...  50.6 us
    pallas_call x1, Pallas kernels, dispatch(): pl.pallas_call(functools.partial(dispatch_kernel, count), out_shape=(full...  41.6 us
    pallas_call x1, Pallas kernels, module(): pl.pallas_call(functools.partial(module_kernel, count), out_shape=(jax.Sh...  16.4 us
    slice x1, local copies, waits for them, and re-layouts, kernel_shards(): grads[2:3]  6.07 us
    dot_general x3, matrix products, contract_cols(): lax.dot_general(left, right, (((1,), (1,)), ((), ())), preferred_element_...  5.58 us
    unnamed x34, local copies, waits for them, and re-layouts  4.9 us
    dot_general x4, matrix products, contract_rows(): lax.dot_general(left, right, (((0,), (0,)), ((), ())), preferred_element_...  4.38 us

commit v1 on v0

--- a/solution.py
+++ b/solution.py
@@ -356,29 +356,47 @@
     cot,
     pick,
     proj,
+    conv_out,
+    row_mean,
+    row_rstd,
+    gain,
+    taps,
     hidden,
     gate_delta,
     up_delta,
     expert_in,
     expert_cot,
-    stream,
-    proj_out,
+    mine_out,
+    unit_out,
+    columns,
     grads,
     landed,
     middle,
     reduced,
     back,
+    stream,
+    proj_all,
+    sums,
+    arrived,
+    extended,
     send,
     recv,
     back_send,
     back_recv,
     wide_send,
     wide_recv,
+    strip_send,
+    strip_recv,
+    strip_local,
+    sum_send,
+    sum_recv,
+    edge_send,
+    edge_recv,
     *proj_sems,
 ):
     me, tp = lax.axis_index("sp"), lax.axis_index("tp")
     capacity, width = reduced.shape[1:]
-    units = hidden.shape[0]
+    tokens, channels = conv_out.shape
     across, down, corner = tp + 1 - 2 * (tp % 2), (tp + 2) % 4, 3 - tp
     group = (across, down, corner)
     others = [(me + d) % count for d in range(1, count)]
@@ -451,31 +469,33 @@
         else:
             back[pl.ds(pl.multiple_of(me * capacity, capacity), capacity), :] = total
 
-    pieces = 4 if units % 64 == 0 else 1
-    tile = units // pieces
-    spots = pieces * 4
     products = ((gate_delta, expert_in), (up_delta, expert_in), (hidden, expert_cot))
+    piece = PIECE if width % PIECE == 0 else width
 
     def product(spot, carry):
-        rows = pl.ds(pl.multiple_of(spot // 4 * tile, 16), tile)
-        columns = pl.ds(pl.multiple_of(spot % 4 * width, 128), width)
+        spots = pl.ds(pl.multiple_of(spot * piece, 128), piece)
         for a, (left, right) in enumerate(products):
-            value = jnp.dot(
-                left[rows, :], right[:, columns], preferred_element_type=jnp.float32
-            )
-            grads[a, rows, columns] = value.astype(jnp.bfloat16)
+            value = jnp.dot(left[...], right[:, spots], preferred_element_type=jnp.float32)
+            grads[a, :, spots] = value.astype(jnp.bfloat16)
         return carry
 
-    window = min(3, count)
+    pieces = 4 * width // piece
+    window = min(WINDOW, count)
     for step in range(window):
         begin(step)
-    gather = ChipGather(proj, proj_out, proj_sems, me, tp, count)
+    gather = ChipGather(proj, proj_all, proj_sems, me, tp, count)
     gather.start()
+    rstd = jnp.broadcast_to(row_rstd[...], (tokens, tokens)).T[:, 0:1]
+    mean = jnp.broadcast_to(row_mean[...], (tokens, tokens)).T[:, 0:1]
+    normed = (conv_out[...].astype(jnp.float32) - mean) * rstd
+    scaled = normed * gain[...]
+    sig = jax.nn.sigmoid(scaled)
+    slope = sig * (1.0 + scaled * (1.0 - sig)) * gain[...]
     for step in range(count):
-        lax.fori_loop(spots * step // count, spots * (step + 1) // count, product, 0)
+        lax.fori_loop(pieces * step // count, pieces * (step + 1) // count, product, 0)
+        forward(step)
         if step + window < count:
             begin(step + window)
-        forward(step)
         if step >= 1:
             settle(step - 1)
     settle(count - 1)
@@ -490,97 +510,34 @@
             tp,
         ).wait_recv()
     mine = jnp.dot(pick[...], back[...], preferred_element_type=jnp.float32)
-    columns = pl.ds(pl.multiple_of(tp * width, 128), width)
-    stream[:, columns] = (cot[...].astype(jnp.float32) + mine).astype(jnp.bfloat16)
+    mine_out[...] = mine
+
+    def quarter(index):
+        return pl.ds(pl.multiple_of(index * width, 128), width)
+
+    stream[:, quarter(tp)] = (cot[...].astype(jnp.float32) + mine).astype(jnp.bfloat16)
 
     def wide_copy(q):
-        spot = stream.at[:, columns]
+        spot = stream.at[:, quarter(tp)]
         return remote(spot, spot, wide_send.at[q], wide_recv.at[q], me, group[q])
 
     for q in range(3):
         wide_copy(q).start()
+    gather.finish()
+
+    def part(index):
+        return jnp.dot(
+            stream[:, quarter(index)],
+            proj_all[quarter(index), :],
+            preferred_element_type=jnp.float32,
+        )
+
+    mixed_grad = part(tp)
     for q in range(3):
-        wide_copy(q).wait()
-    for step in range(count):
-        share_copy(step, 0).wait_send()
-        share_copy(step, 1).wait_send()
-        middle_copy(step).wait_send()
-    for other in others:
-        back_copy(other).wait_send()
-    gather.finish()
-
-
-def combine(partial_value, cot, pick, proj, hidden, gate_delta, up_delta, rows, rows_cot, count):
-    tokens, width = cot.shape
-    capacity = partial_value.shape[0] // count
-    return pl.pallas_call(
-        functools.partial(combine_kernel, count),
-        out_shape=(
-            jax.ShapeDtypeStruct((tokens, partial_value.shape[1]), jnp.bfloat16),
-            jax.ShapeDtypeStruct((count * proj.shape[0], proj.shape[1]), jnp.bfloat16),
-            jax.ShapeDtypeStruct((3, hidden.shape[0], partial_value.shape[1]), jnp.bfloat16),
-        ),
-        in_specs=[VMEM] * 9,
-        out_specs=(VMEM,) * 3,
-        scratch_shapes=[
-            pltpu.VMEM((3, count, capacity, width), jnp.bfloat16),
-            pltpu.VMEM((count, capacity, width), jnp.bfloat16),
-            pltpu.VMEM((count, capacity, width), jnp.bfloat16),
-            pltpu.VMEM((count * capacity, width), jnp.bfloat16),
-            pltpu.SemaphoreType.DMA((count, 3)),
-            pltpu.SemaphoreType.DMA((count, 3)),
-            pltpu.SemaphoreType.DMA((count,)),
-            pltpu.SemaphoreType.DMA((count,)),
-            pltpu.SemaphoreType.DMA((3,)),
-            pltpu.SemaphoreType.DMA((3,)),
-        ]
-        + gather_sems(count),
-        compiler_params=pltpu.CompilerParams(
-            collective_id=1, has_side_effects=True, vmem_limit_bytes=40 << 20
-        ),
-        name="combine",
-        cost_estimate=pl.CostEstimate(
-            flops=6 * hidden.size * partial_value.shape[1],
-            bytes_accessed=50 * partial_value.size * 2,
-            transcendentals=0,
-        ),
-    )(partial_value, cot, pick, proj, hidden, gate_delta, up_delta, rows, rows_cot)
-
-
-def module_kernel(
-    count,
-    stream,
-    proj,
-    mixed,
-    conv_out,
-    row_mean,
-    row_rstd,
-    gain,
-    taps,
-    v_value,
-    v_gate,
-    proj_grad,
-    value_grad,
-    gating_grad,
-    columns,
-    sums,
-    arrived,
-    extended,
-    send,
-    recv,
-    local,
-    sum_send,
-    sum_recv,
-    edge_send,
-    edge_recv,
-):
-    me, tp = lax.axis_index("sp"), lax.axis_index("tp")
-    tokens, channels = conv_out.shape
+        spot = stream.at[:, quarter(group[q])]
+        remote(spot, spot, wide_send.at[q], wide_recv.at[q], me, group[q]).wait_recv()
+        mixed_grad = mixed_grad + part(group[q])
     depth = stream.shape[1] // count
-    halo = extended.shape[0] - tokens
-    group = (tp + 1 - 2 * (tp % 2), (tp + 2) % 4, 3 - tp)
-    others = [(me + d) % count for d in range(1, count)]
-    greet([(other, tp) for other in others] + [(me, other) for other in group])
 
     def strip(index):
         return stream.at[:, pl.ds(pl.multiple_of(index * depth, 128), depth)]
@@ -589,23 +546,13 @@
         return remote(
             strip(target),
             rows_of(columns, me, tokens),
-            send.at[target],
-            recv.at[me],
+            strip_send.at[target],
+            strip_recv.at[me],
             target,
             tp,
         )
 
-    own = pltpu.make_async_copy(strip(me), rows_of(columns, me, tokens), local)
-    own.start()
-    for other in others:
-        strip_copy(other).start()
-    mixed_grad = jnp.dot(stream[...], proj[...], preferred_element_type=jnp.float32)
-    rstd = jnp.broadcast_to(row_rstd[...], (tokens, tokens)).T[:, 0:1]
-    mean = jnp.broadcast_to(row_mean[...], (tokens, tokens)).T[:, 0:1]
-    normed = (conv_out[...].astype(jnp.float32) - mean) * rstd
-    scaled = normed * gain[...]
-    sig = jax.nn.sigmoid(scaled)
-    norm_grad = mixed_grad * sig * (1.0 + scaled * (1.0 - sig)) * gain[...]
+    norm_grad = mixed_grad * slope
     first = jnp.sum(norm_grad, axis=1, keepdims=True)
     second = jnp.sum(norm_grad * normed, axis=1, keepdims=True)
     lanes = lax.broadcasted_iota(jnp.int32, (tokens, 128), 1)
@@ -617,8 +564,10 @@
 
     for q in range(3):
         sum_copy(q).start()
-    value_sig = jax.nn.sigmoid(v_gate[...].astype(jnp.float32))
-    gating_scale = v_value[...].astype(jnp.float32) * value_sig * (1.0 - value_sig)
+    own = pltpu.make_async_copy(strip(me), rows_of(columns, me, tokens), strip_local)
+    own.start()
+    for other in others:
+        strip_copy(other).start()
     for q in range(3):
         sum_copy(q).wait()
     total = sums[...] + arrived[0] + arrived[1] + arrived[2]
@@ -626,6 +575,7 @@
     means = jnp.concatenate([total] * 16, axis=0).T
     conv_grad = rstd * (norm_grad - means[:, 0:1] - normed * means[:, 1:2])
     extended[:tokens] = conv_grad
+    halo = extended.shape[0] - tokens
     edge = remote(
         extended.at[pl.ds(0, halo)],
         extended.at[pl.ds(tokens, halo)],
@@ -653,20 +603,25 @@
         lead = kernel - 1 - offset
         tap = taps[offset : offset + 1, :].astype(jnp.float32)
         unit_grad = unit_grad + tap * extended[lead : lead + tokens, :]
-    value_grad[...] = (unit_grad * value_sig).astype(jnp.bfloat16)
-    gating_grad[...] = (unit_grad * gating_scale).astype(jnp.bfloat16)
+    unit_out[...] = unit_grad
     own.wait()
     for other in others:
         remote(
             strip(other),
             rows_of(columns, other, tokens),
-            send.at[other],
-            recv.at[other],
+            strip_send.at[other],
+            strip_recv.at[other],
             other,
             tp,
         ).wait_recv()
-    proj_grad[...] = contract_rows(columns[...], mixed[...])
+    for q in range(3):
+        wide_copy(q).wait_send()
+    for step in range(count):
+        share_copy(step, 0).wait_send()
+        share_copy(step, 1).wait_send()
+        middle_copy(step).wait_send()
     for other in others:
+        back_copy(other).wait_send()
         strip_copy(other).wait_send()
 
     @pl.when(me > 0)
@@ -674,37 +629,151 @@
         edge.wait_send()
 
 
-def module(stream, proj, mixed, conv_out, row_mean, row_rstd, gain, taps, v_value, v_gate, count):
-    tokens, channels = conv_out.shape
-    depth = stream.shape[1] // count
+WINDOW = 3
+PIECE = 256
+
+
+def combine(
+    partial_value, cot, pick, proj, conv_out, row_mean, row_rstd, gain, taps, acts, count
+):
+    tokens, width = cot.shape
+    channels = conv_out.shape[1]
+    capacity = partial_value.shape[0] // count
+    full = partial_value.shape[1]
+    depth = full // count
     halo = -(-(taps.shape[0] - 1) // 8) * 8
+    dma = pltpu.SemaphoreType.DMA
     return pl.pallas_call(
-        functools.partial(module_kernel, count),
+        functools.partial(combine_kernel, count),
         out_shape=(
-            jax.ShapeDtypeStruct((depth, channels), jnp.float32),
-            jax.ShapeDtypeStruct((tokens, channels), jnp.bfloat16),
-            jax.ShapeDtypeStruct((tokens, channels), jnp.bfloat16),
+            jax.ShapeDtypeStruct((tokens, width), jnp.float32),
+            jax.ShapeDtypeStruct((tokens, channels), jnp.float32),
+            jax.ShapeDtypeStruct((count * tokens, depth), jnp.bfloat16),
+            jax.ShapeDtypeStruct((3, acts[0].shape[0], full), jnp.bfloat16),
         ),
-        in_specs=[VMEM] * 10,
-        out_specs=(VMEM,) * 3,
+        in_specs=[VMEM] * 14,
+        out_specs=(VMEM,) * 4,
         scratch_shapes=[
-            pltpu.VMEM((count * tokens, depth), jnp.bfloat16),
+            pltpu.VMEM((3, count, capacity, width), jnp.bfloat16),
+            pltpu.VMEM((count, capacity, width), jnp.bfloat16),
+            pltpu.VMEM((count, capacity, width), jnp.bfloat16),
+            pltpu.VMEM((count * capacity, width), jnp.bfloat16),
+            pltpu.VMEM((tokens, full), jnp.bfloat16),
+            pltpu.VMEM((count * proj.shape[0], proj.shape[1]), jnp.bfloat16),
             pltpu.VMEM((8, tokens), jnp.float32),
             pltpu.VMEM((3, 8, tokens), jnp.float32),
             pltpu.VMEM((tokens + halo, channels), jnp.float32),
-            pltpu.SemaphoreType.DMA((count,)),
-            pltpu.SemaphoreType.DMA((count,)),
-            pltpu.SemaphoreType.DMA,
-            pltpu.SemaphoreType.DMA((3,)),
-            pltpu.SemaphoreType.DMA((3,)),
-            pltpu.SemaphoreType.DMA,
-            pltpu.SemaphoreType.DMA,
+            dma((count, 3)),
+            dma((count, 3)),
+            dma((count,)),
+            dma((count,)),
+            dma((3,)),
+            dma((3,)),
+            dma((count,)),
+            dma((count,)),
+            dma,
+            dma((3,)),
+            dma((3,)),
+            dma,
+            dma,
+        ]
+        + gather_sems(count),
+        compiler_params=pltpu.CompilerParams(
+            collective_id=1, has_side_effects=True, vmem_limit_bytes=24 << 20
+        ),
+        name="combine",
+        cost_estimate=pl.CostEstimate(
+            flops=2 * tokens * full * channels,
+            bytes_accessed=50 * partial_value.size * 2,
+            transcendentals=0,
+        ),
+    )(partial_value, cot, pick, proj, conv_out, row_mean, row_rstd, gain, taps, *acts)
+
+
+def finish_kernel(
+    grads,
+    mine,
+    unit_grad,
+    columns,
+    mixed,
+    cot,
+    v_value,
+    v_gate,
+    gate_out,
+    up_out,
+    down_out,
+    proj_out,
+    stream_out,
+    value_out,
+    gating_out,
+    proj,
+    stream,
+    value,
+    gating,
+    sems,
+):
+    half = grads.shape[1] // 2
+    copies = []
+    for a, out in enumerate((gate_out, up_out, down_out)):
+        for part in range(2):
+            rows = pl.ds(part * half, half)
+            copies.append(
+                pltpu.make_async_copy(grads.at[a, rows], out.at[0, rows], sems.at[2 * a + part])
+            )
+    for copy in copies:
+        copy.start()
+
+    def put(local, out, index):
+        copy = pltpu.make_async_copy(local, out, sems.at[index])
+        copy.start()
+        copies.append(copy)
+
+    stream[...] = (cot[...].astype(jnp.float32) + mine[...]).astype(jnp.bfloat16)
+    put(stream, stream_out, 6)
+    unit = unit_grad[...]
+    value_sig = jax.nn.sigmoid(v_gate[...].astype(jnp.float32))
+    value[...] = (unit * value_sig).astype(jnp.bfloat16)
+    put(value, value_out, 7)
+    gating[...] = (unit * v_value[...].astype(jnp.float32) * value_sig * (1.0 - value_sig)).astype(
+        jnp.bfloat16
+    )
+    put(gating, gating_out, 8)
+    proj[...] = contract_rows(columns[...], mixed[...])
+    put(proj, proj_out, 9)
+    for copy in copies:
+        copy.wait()
+
+
+def finish(grads, mine, unit_grad, columns, mixed, cot, v_value, v_gate):
+    shape = (1,) + grads.shape[1:]
+    anywhere = pl.BlockSpec(memory_space=pl.ANY)
+    proj_shape = (columns.shape[1], mixed.shape[1])
+    return pl.pallas_call(
+        finish_kernel,
+        out_shape=tuple(jax.ShapeDtypeStruct(shape, jnp.bfloat16) for _ in range(3))
+        + (
+            jax.ShapeDtypeStruct(proj_shape, jnp.float32),
+            jax.ShapeDtypeStruct(cot.shape, jnp.bfloat16),
+            jax.ShapeDtypeStruct(v_value.shape, jnp.bfloat16),
+            jax.ShapeDtypeStruct(v_value.shape, jnp.bfloat16),
+        ),
+        in_specs=[VMEM] * 8,
+        out_specs=(anywhere,) * 7,
+        scratch_shapes=[
+            pltpu.VMEM(proj_shape, jnp.float32),
+            pltpu.VMEM(cot.shape, jnp.bfloat16),
+            pltpu.VMEM(v_value.shape, jnp.bfloat16),
+            pltpu.VMEM(v_value.shape, jnp.bfloat16),
+            pltpu.SemaphoreType.DMA((10,)),
         ],
-        compiler_params=pltpu.CompilerParams(
-            collective_id=2, has_side_effects=True, vmem_limit_bytes=40 << 20
+        compiler_params=pltpu.CompilerParams(vmem_limit_bytes=24 << 20),
+        name="finish",
+        cost_estimate=pl.CostEstimate(
+            flops=2 * columns.size * mixed.shape[1],
+            bytes_accessed=2 * grads.size * 2,
+            transcendentals=0,
         ),
-        name="module",
-    )(stream, proj, mixed, conv_out, row_mean, row_rstd, gain, taps, v_value, v_gate)
+    )(grads, mine, unit_grad, columns, mixed, cot, v_value, v_gate)
 
 
 def kernel_shards(
@@ -776,33 +845,20 @@
     )
     up_delta = (hidden_grad * gate_act).astype(jnp.bfloat16)
     partial_value = contract_rows(gate_delta, gate_w) + contract_rows(up_delta, up_w)
-    stream_full, proj_full, grads = combine(
+    mine, unit_grad, columns, grads = combine(
         partial_value.astype(jnp.bfloat16),
         cotangent,
         pick,
         out_proj,
-        hidden,
-        gate_delta,
-        up_delta,
-        expert_in,
-        expert_cot,
-        experts,
-    )
-    proj_g, value_g, gating_g = module(
-        stream_full,
-        proj_full,
-        mixed_all,
         conv_out,
         row_mean[None, :],
         row_rstd[None, :],
         ln_gain[None, :],
         taps,
-        v_value,
-        v_gate,
+        (hidden, gate_delta, up_delta, expert_in, expert_cot),
         experts,
     )
-    stream = lax.dynamic_slice_in_dim(stream_full, lax.axis_index("tp") * width, width, 1)
-    return (grads[0:1], grads[1:2], grads[2:3], proj_g, stream, value_g, gating_g)
+    return finish(grads, mine, unit_grad, columns, mixed_all, cotangent, v_value, v_gate)
 
 
 def shards(*blocks):

time: 135 us -> 120 us (0.89)
  local copies, waits for them, and re-layouts: 12.7 us -> 2.26 us
  Pallas kernels: 109 us -> 103 us
    pallas_call x1, Pallas kernels: 16.4 us -> 3.73 us  [finish(): pl.pallas_call(finish_kernel, out_shape=tuple((jax.ShapeDtypeStruct(shape...]
    pallas_call x1, Pallas kernels: 50.6 us -> 57.2 us  [combine(): pl.pallas_call(functools.partial(combine_kernel, count), out_shape=(jax.S...]
    slice x1 -> x0, local copies, waits for them, and re-layouts: 6.07 us -> none  [kernel_shards(): grads[2:3]]
    unnamed x34 -> x27, local copies, waits for them, and re-layouts: 4.9 us -> 1.05 us
where the time goes in v1:
time: 120 us
  Pallas kernels  103 us (86%)
  matrix products  10.5 us (9%)
  other arithmetic  3.12 us (3%)
  local copies, waits for them, and re-layouts  2.26 us (2%)
    pallas_call x1, Pallas kernels, combine(): pl.pallas_call(functools.partial(combine_kernel, count), out_shape=(jax.S...  57.2 us
    pallas_call x1, Pallas kernels, dispatch(): pl.pallas_call(functools.partial(dispatch_kernel, count), out_shape=(full...  41.6 us
    dot_general x3, matrix products, contract_cols(): lax.dot_general(left, right, (((1,), (1,)), ((), ())), preferred_element_...  5.71 us
    dot_general x4, matrix products, contract_rows(): lax.dot_general(left, right, (((0,), (0,)), ((), ())), preferred_element_...  4.56 us
    pallas_call x1, Pallas kernels, finish(): pl.pallas_call(finish_kernel, out_shape=tuple((jax.ShapeDtypeStruct(shape...  3.73 us

profile of v1, /device:TPU:9, one launch (start us, length us, event | category | flops | bytes accessed | tf_op | source)
XLA Modules:
  0.0 119.6 jit_solution(12444834536250983268)
XLA Ops:
  0.6 0.0 copy-start
  0.6 0.0 copy-start.11
  0.7 0.9 slice_bitcast_fusion.1
  1.5 0.9 copy.28
  2.4 0.1 eq.45
  2.5 0.2 fusion.19
  2.7 0.1 convert_element_type.56
  2.9 0.1 copy.29
  2.9 0.0 copy-start.12
  2.9 0.9 multiply_add_fusion
  3.8 1.0 multiply_convert_fusion.3.mixed
  4.8 0.1 fusion.30.pick
  5.0 1.0 fusion.20
  6.0 0.1 fusion.28
  6.1 0.3 convolution_convert_fusion
  6.4 0.0 copy-done.11
  6.4 0.4 convolution_convert_fusion.1
  6.8 41.6 %dispatch.1 = (bf16[512,2048]{1,0:T(8,128)(2,1)S(1)}, bf16[512,2048]{1,0:T(8,128)(2,1)S(1)}, bf16[1024,256]{1,0:T(8,128)(2,1)S(1)}) custom-call(bf16[8,64,512]{2,1,0:T(8,128)(2,1)S(1)} %bitcast.46, bf16[8,64,512]{2,1,0:T(8,128)(2,1)S(1)} %bitcast.47, bf16[128,256]{1,0:T(8,128)(2,1)S(1)} %multiply_convert_fusion.3.mixed), custom_call_target="tpu_custom_call" | custom-call | bytes 104857600 | tf_op jit(solution)/shard_map/dispatch/pallas_call | solution.py:328
  48.5 0.0 copy-done.12
  48.5 0.0 copy-start.10
  48.5 1.7 %fusion.9 = f32[704,512]{1,0:T(8,128)S(1)} fusion(bf16[512,2048]{1,0:T(8,128)(2,1)S(1)} %get-tuple-element.14.expert_cot, bf16[1,704,2048]{2,1,0:T(8,128)(2,1)S(1)} %copy-done.12), kind=kOutput, calls=%fused_computation.10 | convolution fusion | flops 1476395008 | bytes 6422528 | tf_op jit(solution)/shard_map/dot_general | solution.py:34
  50.2 0.1 copy-done.10
  50.3 1.8 %fusion.15 = f32[704,512]{1,0:T(8,128)S(1)} fusion(bf16[512,2048]{1,0:T(8,128)(2,1)S(1)} %get-tuple-element.15.expert_in, bf16[1,704,2048]{2,1,0:T(8,128)(2,1)S(1)} %copy-done.10), kind=kOutput, calls=%fused_computation.12 | convolution fusion | flops 1476395008 | bytes 6422528 | tf_op jit(solution)/shard_map/dot_general | solution.py:34
  52.1 0.0 copy-done
  52.1 2.3 %multiply_convert_fusion = (bf16[704,512]{1,0:T(8,128)(2,1)S(1)}, bf16[704,512]{1,0:T(8,128)(2,1)S(1)}, bf16[704,512]{1,0:T(8,128)(2,1)S(1)}) fusion(f32[704,512]{1,0:T(8,128)S(1)} %fusion.15, f32[704,512]{1,0:T(8,128)S(1)} %fusion.9, bf16[512,2048]{1,0:T(8,128)(2,1)S(1)} %get-tuple-element.15.expert_in, bf16[1,704,2048]{2,1,0:T(8,128)(2,1)S(1)} %copy-done), kind=kOutput, calls=%fused_computation.13 | convolution fusion | flops 1481801728 | bytes 10027008 | tf_op jit(solution)/shard_map/dot_general | solution.py:34
  54.4 1.9 %fusion = f32[512,2048]{1,0:T(8,128)S(1)} fusion(bf16[704,512]{1,0:T(8,128)(2,1)S(1)} %get-tuple-element.22.gate_delta, bf16[1,704,2048]{2,1,0:T(8,128)(2,1)S(1)} %copy-done.10), kind=kOutput, calls=%fused_computation.1 | convolution fusion | flops 1476395008 | bytes 7798784 | tf_op jit(solution)/shard_map/dot_general | solution.py:28
  56.2 0.0 copy-start.1
  56.2 0.0 copy-start.2
  56.2 0.0 copy-start.3
  56.3 0.0 copy-start.6
  56.3 0.0 copy-start.7
  56.3 0.0 copy-start.8
  56.3 0.0 copy-start.9
  56.3 2.0 %add_convert_fusion.partial_ref = bf16[512,2048]{1,0:T(8,128)(2,1)S(1)} fusion(f32[512,2048]{1,0:T(8,128)S(1)} %fusion, bf16[704,512]{1,0:T(8,128)(2,1)S(1)} %get-tuple-element.23.up_delta, bf16[1,704,2048]{2,1,0:T(8,128)(2,1)S(1)} %copy-done), kind=kOutput, calls=%fused_computation | convolution fusion | flops 1478492160 | bytes 9895936 | tf_op jit(solution)/shard_map/dot_general | solution.py:28
  58.3 0.0 copy-done.1
  58.3 0.0 copy-done.2
  58.3 0.0 copy-done.3
  58.3 0.0 copy-done.6
  58.3 0.0 copy-done.7
  58.4 0.0 copy-done.8
  58.4 0.0 copy-done.9
  58.4 0.0 copy-start.4
  58.4 0.0 copy-start.5
  58.4 57.2 %combine.1 = (f32[128,512]{1,0:T(8,128)S(1)}, f32[128,256]{1,0:T(8,128)S(1)}, bf16[1024,256]{1,0:T(8,128)(2,1)S(1)}, bf16[3,704,2048]{2,1,0:T(8,128)(2,1)S(1)}) custom-call(bf16[512,2048]{1,0:T(8,128)(2,1)S(1)} %add_convert_fusion.partial_ref, bf16[128,512]{1,0:T(8,128)(2,1)S(1)} %copy-done.1, bf16[128,512]{1,0:T(8,128)(2,1)S(1)} %fusion.30.pick, ...), custom_call_target="tpu_custom_call" | custom-call | flops 134217728 | bytes 104857600 | tf_op jit(solution)/shard_map/combine/pallas_call | solution.py:646
  115.7 0.0 copy-done.4
  115.7 0.0 copy-done.5
  115.7 3.7 %finish.1 = (bf16[1,704,2048]{2,1,0:T(8,128)(2,1)}, bf16[1,704,2048]{2,1,0:T(8,128)(2,1)}, bf16[1,704,2048]{2,1,0:T(8,128)(2,1)}, f32[256,256]{1,0:T(8,128)}, bf...) custom-call(bf16[3,704,2048]{2,1,0:T(8,128)(2,1)S(1)} %get-tuple-element.16.grads, ...), custom_call_target="tpu_custom_call" | custom-call | flops 134217728 | bytes 17301504 | tf_op jit(solution)/shard_map/finish/pallas_call | solution.py:751
  (2 shorter events, 0.0 us)
Async XLA Ops:
  0.6 51.5 %copy-start = (bf16[1,704,2048]{2,1,0:T(8,128)(2,1)S(1)}, bf16[1,704,2048]{2,1,0:T(8,128)(2,1)}, u32[]{:S(2)}) copy-start(bf16[1,704,2048]{2,1,0:T(8,128)(2,1)} %param.20) | copy-start | bytes 8650756
  0.6 5.8 %copy-start.11 = (bf16[128,512]{1,0:T(8,128)(2,1)S(1)}, bf16[128,512]{1,0:T(8,128)(2,1)}, u32[]{:S(2)}) copy-start(bf16[128,512]{1,0:T(8,128)(2,1)} %param.15) | copy-start | bytes 393220
  2.9 45.5 %copy-start.12 = (bf16[1,704,2048]{2,1,0:T(8,128)(2,1)S(1)}, bf16[1,704,2048]{2,1,0:T(8,128)(2,1)}, u32[]{:S(2)}) copy-start(bf16[1,704,2048]{2,1,0:T(8,128)(2,1)} %param.21) | copy-start | bytes 8650756
  48.5 1.8 %copy-start.10 = (bf16[1,704,2048]{2,1,0:T(8,128)(2,1)S(1)}, bf16[1,704,2048]{2,1,0:T(8,128)(2,1)}, u32[]{:S(2)}) copy-start(bf16[1,704,2048]{2,1,0:T(8,128)(2,1)} %param.19) | copy-start | bytes 8650756
  56.2 2.1 %copy-start.1 = (bf16[128,512]{1,0:T(8,128)(2,1)S(1)}, bf16[128,512]{1,0:T(8,128)(2,1)}, u32[]{:S(2)}) copy-start(bf16[128,512]{1,0:T(8,128)(2,1)} %cot.3) | copy-start | bytes 393220
  56.2 2.1 %copy-start.2 = (bf16[128,256]{1,0:T(8,128)(2,1)S(1)}, bf16[128,256]{1,0:T(8,128)(2,1)}, u32[]{:S(2)}) copy-start(bf16[128,256]{1,0:T(8,128)(2,1)} %conv_out.1) | copy-start | bytes 196612
  56.2 2.1 %copy-start.3 = (bf16[256,256]{1,0:T(8,128)(2,1)S(1)}, bf16[256,256]{1,0:T(8,128)(2,1)}, u32[]{:S(2)}) copy-start(bf16[256,256]{1,0:T(8,128)(2,1)} %proj.1) | copy-start | bytes 393220
  56.3 2.1 %copy-start.6 = (bf16[31,256]{1,0:T(8,128)(2,1)S(1)}, bf16[31,256]{1,0:T(8,128)(2,1)}, u32[]{:S(2)}) copy-start(bf16[31,256]{1,0:T(8,128)(2,1)} %taps.1) | copy-start | bytes 47620
  56.3 2.1 %copy-start.7 = (f32[256]{0:T(256)S(1)}, f32[256]{0:T(256)}, u32[]{:S(2)}) copy-start(f32[256]{0:T(256)} %param.27) | copy-start | bytes 3076
  56.3 2.1 %copy-start.8 = (f32[128]{0:T(128)S(1)}, f32[128]{0:T(128)}, u32[]{:S(2)}) copy-start(f32[128]{0:T(128)} %param.26) | copy-start | bytes 1540
  56.3 2.1 %copy-start.9 = (f32[128]{0:T(128)S(1)}, f32[128]{0:T(128)}, u32[]{:S(2)}) copy-start(f32[128]{0:T(128)} %param.25) | copy-start | bytes 1540
  58.4 57.3 %copy-start.4 = (bf16[128,256]{1,0:T(8,128)(2,1)S(1)}, bf16[128,256]{1,0:T(8,128)(2,1)}, u32[]{:S(2)}) copy-start(bf16[128,256]{1,0:T(8,128)(2,1)} %v_value.1) | copy-start | bytes 196612
  58.4 57.3 %copy-start.5 = (bf16[128,256]{1,0:T(8,128)(2,1)S(1)}, bf16[128,256]{1,0:T(8,128)(2,1)}, u32[]{:S(2)}) copy-start(bf16[128,256]{1,0:T(8,128)(2,1)} %v_gate.1) | copy-start | bytes 196612

commit v2 on v1

--- a/solution.py
+++ b/solution.py
@@ -182,180 +182,387 @@
     return ref.at[pl.ds(pl.multiple_of(index * count, count), count)]
 
 
-class ChipGather:
-    def __init__(self, own, everyone, sems, me, tp, count):
-        self.own, self.everyone, self.me, self.tp, self.count = own, everyone, me, tp, count
-        self.send, self.recv, self.relay, self.local = sems
-        self.partner = me + 1 - 2 * (me % 2)
-        self.ahead = [(me + 2 * e) % count for e in range(1, count // 2)]
-        self.behind = [(me + count - 2 * e) % count for e in range(1, count // 2)]
-
-    def block(self, index):
-        return rows_of(self.everyone, index, self.own.shape[0])
-
-    def first(self, target):
-        return remote(
-            self.own,
-            self.block(self.me),
-            self.send.at[target],
-            self.recv.at[self.me],
-            target,
-            self.tp,
-        )
-
-    def onward(self, origin):
-        return remote(
-            self.block(origin),
-            self.block(origin),
-            self.relay.at[origin],
-            self.recv.at[origin],
-            self.partner,
-            self.tp,
-        )
-
-    def start(self):
-        pltpu.make_async_copy(self.own, self.block(self.me), self.local).start()
-        for target in self.ahead + [self.partner]:
-            self.first(target).start()
-
-    def pass_on(self):
-        for origin in self.behind:
-            self.onward(origin).wait_recv()
-            self.onward(origin).start()
-
-    def finish(self):
-        pltpu.make_async_copy(self.own, self.block(self.me), self.local).wait()
-        for step in range(self.count // 2):
-            origin = (self.partner + 2 * step) % self.count
-            self.onward(origin).wait_recv()
-        for target in self.ahead + [self.partner]:
-            self.first(target).wait_send()
-        for origin in self.behind:
-            self.onward(origin).wait_send()
-
-
-def gather_sems(count):
-    return [
-        pltpu.SemaphoreType.DMA((count,)),
-        pltpu.SemaphoreType.DMA((count,)),
-        pltpu.SemaphoreType.DMA((count,)),
-        pltpu.SemaphoreType.DMA,
-    ]
+def announce(peers):
+    barrier = pltpu.get_barrier_semaphore()
+    for sp, tp in peers:
+        pl.semaphore_signal(
+            barrier, inc=1, device_id={"sp": sp, "tp": tp}, device_id_type=pl.DeviceIdType.MESH
+        )
+
+
+def nearby(z, chips, j):
+    high = 2 * z // chips
+    near = (1 - high) * z + high * (chips - 1 - z)
+    both = (2 * near - j + 2 * chips) // (2 * chips)
+    hop = (j + 1) // 2
+    two = z - hop if j % 2 == 1 else z + hop
+    one = z + (1 - 2 * high) * (j - near)
+    return both * two + (1 - both) * one
 
 
 def dispatch_kernel(
-    count, rows, cot, mixed, rows_out, cot_out, mixed_out, send, recv, local, *mixed_sems
+    count,
+    x,
+    cot,
+    routes_far,
+    weights_far,
+    conv_far,
+    mean_far,
+    rstd_far,
+    gain_far,
+    proj,
+    rows_out,
+    cot_out,
+    mixed_all,
+    proj_all,
+    meta,
+    tok_x,
+    tok_c,
+    metas,
+    routes,
+    weights,
+    conv_out,
+    row_mean,
+    row_rstd,
+    gain,
+    load,
+    z_send,
+    z_recv,
+    side_send,
+    side_recv,
+    relay_send,
+    relay_recv,
+    push_send,
+    push_recv,
+    meta_send,
+    meta_recv,
 ):
     me, tp = lax.axis_index("sp"), lax.axis_index("tp")
-    capacity, width = rows.shape[1:]
+    tokens, width = x.shape
+    capacity = rows_out.shape[0] // count
+    chips = count // 2
+    z, lane = me // 2, me % 2
+    partner = me + 1 - 2 * lane
     across, down, corner = tp + 1 - 2 * (tp % 2), (tp + 2) % 4, 3 - tp
     others = [(me + d) % count for d in range(1, count)]
-    greet([(other, tp) for other in others] + [(me, across), (me, down)])
-    arrays = ((rows, rows_out), (cot, cot_out))
+    announce([(other, tp) for other in others] + [(me, across), (me, down)])
+    half = tokens // 2
+    toks = (tok_x, tok_c)
+    gathered = (mixed_all, proj_all)
+
+    def columns(index):
+        return pl.ds(pl.multiple_of(index * width, 128), width)
 
     def block(a, source, owner):
-        return arrays[a][1].at[
-            pl.ds(pl.multiple_of(source * capacity, capacity), capacity),
-            pl.ds(pl.multiple_of(owner * width, 128), width),
-        ]
-
-    def own_copy(a):
-        return pltpu.make_async_copy(arrays[a][0].at[me], block(a, me, tp), local.at[a])
-
-    def out_copy(a, target):
+        return toks[a].at[source, :, columns(owner)]
+
+    loads = [
+        pltpu.make_async_copy(far, near, load.at[index])
+        for index, (far, near) in enumerate(
+            (
+                (x, block(0, me, tp)),
+                (cot, block(1, me, tp)),
+                (routes_far, routes),
+                (weights_far, weights),
+                (conv_far, conv_out),
+                (mean_far, row_mean),
+                (rstd_far, row_rstd),
+                (gain_far, gain),
+                (proj, rows_of(proj_all, me, proj.shape[0])),
+            )
+        )
+    ]
+    for copy in loads:
+        copy.start()
+    for copy in loads:
+        copy.wait()
+    rstd = jnp.broadcast_to(row_rstd[...], (tokens, tokens)).T[:, 0:1]
+    mean = jnp.broadcast_to(row_mean[...], (tokens, tokens)).T[:, 0:1]
+    scaled = (conv_out[...].astype(jnp.float32) - mean) * rstd * gain[...]
+    own_mixed = rows_of(mixed_all, me, tokens)
+    own_mixed[...] = (scaled * jax.nn.sigmoid(scaled)).astype(jnp.bfloat16)
+    expert = lax.broadcasted_iota(jnp.int32, (count, tokens), 0)
+    first = routes[0:1, :] == expert
+    second = routes[1:2, :] == expert
+    named = jnp.where(first | second, 1.0, 0.0).astype(jnp.bfloat16)
+    before = lax.broadcasted_iota(jnp.int32, (tokens, tokens), 0) < lax.broadcasted_iota(
+        jnp.int32, (tokens, tokens), 1
+    )
+    before = jnp.where(before, 1.0, 0.0).astype(jnp.bfloat16)
+    earlier = jnp.dot(named, before, preferred_element_type=jnp.float32)
+    spot = earlier + expert.astype(jnp.float32) * capacity
+    spot0 = jnp.sum(jnp.where(first, spot, 0.0), axis=0, keepdims=True)
+    spot1 = jnp.sum(jnp.where(second, spot, 0.0), axis=0, keepdims=True)
+    meta[...] = jnp.concatenate(
+        [spot0, spot1, weights[0:1, :], weights[1:2, :], jnp.zeros((4, tokens), jnp.float32)],
+        axis=0,
+    )
+    metas[me] = meta[...]
+
+    def piece(a, source):
+        if a < 2:
+            return block(a, source, tp)
+        return rows_of(gathered[a - 2], source, gathered[a - 2].shape[0] // count)
+
+    def z_copy(a, o, target, way):
+        spot = piece(a, 2 * o + lane)
         return remote(
-            arrays[a][0].at[target],
-            block(a, me, tp),
-            send.at[a, target, 0],
-            recv.at[a, me, tp],
-            target,
+            spot,
+            spot,
+            z_send.at[a, o, way],
+            z_recv.at[a, o],
+            2 * target + lane,
             tp,
         )
 
-    def side_copy(a, source, owner, target, lane):
-        spot = block(a, source, owner)
-        return remote(spot, spot, send.at[a, source, lane], recv.at[a, source, owner], me, target)
-
+    def way_of(o):
+        return (z - o + chips - 1) // chips
+
+    def z_start(a):
+        for way, bound in ((1, z < chips - 1), (0, z > 0)):
+
+            @pl.when(bound)
+            def _(way=way):
+                z_copy(a, z, z + 2 * way - 1, way).start()
+
+    def z_relay(a, o):
+        way = way_of(o)
+        target = z + 2 * way - 1
+        z_copy(a, o, z, way).wait_recv()
+
+        @pl.when((target >= 0) & (target <= chips - 1))
+        def _():
+            z_copy(a, o, target, way).start()
+
+    def z_finish(a, j):
+        o = nearby(z, chips, j)
+        way = way_of(o)
+        target = z + 2 * way - 1
+
+        @pl.when((target >= 0) & (target <= chips - 1))
+        def _():
+            z_copy(a, o, target, way).wait_send()
+
+    def z_drain(a):
+        for way, bound in ((1, z < chips - 1), (0, z > 0)):
+
+            @pl.when(bound)
+            def _(way=way):
+                z_copy(a, z, z + 2 * way - 1, way).wait_send()
+
+    def side_copy(a, o, side):
+        source = 2 * o + lane
+        spot = block(a, source, tp)
+        return remote(
+            spot,
+            spot,
+            side_send.at[a, o, side],
+            side_recv.at[a, o, side],
+            me,
+            (across, down)[side],
+        )
+
+    def relay_copy(a, o, side):
+        owner, target = ((across, down), (down, across))[side]
+        spot = block(a, 2 * o + lane, owner).at[pl.ds(side * half, half)]
+        return remote(
+            spot, spot, relay_send.at[a, o, side], relay_recv.at[a, o, side], me, target
+        )
+
+    def push_copy(a, o, q, source_lane=None):
+        source = 2 * o + (lane if source_lane is None else source_lane)
+        spot = (
+            block(a, source, (tp, across, down)[q])
+            if q < 3
+            else block(a, source, corner).at[pl.ds((q - 3) * half, half)]
+        )
+        return remote(
+            spot,
+            spot,
+            push_send.at[a, o, q],
+            push_recv.at[a, o, q],
+            partner,
+            tp,
+        )
+
+    def pass_copy(a, o, source_lane=None):
+        spot = piece(a, 2 * o + (lane if source_lane is None else source_lane))
+        return remote(spot, spot, push_send.at[a, o, 0], push_recv.at[a, o, 0], partner, tp)
+
+    def meta_copy(target):
+        return remote(
+            meta, metas.at[me], meta_send.at[target], meta_recv.at[me], target, tp
+        )
+
+    def at(k):
+        j, a = k // 2, k % 2
+        return a, (z if j == 0 else nearby(z, chips, j))
+
+    blocks = 2 * chips
+
+    def spread(k):
+        a, o = at(k)
+        for side in range(2):
+            side_copy(a, o, side).start()
+        push_copy(a, o, 0).start()
+
+    def sides(k):
+        a, o = at(k)
+        for side in range(2):
+            side_copy(a, o, side).wait_recv()
+            relay_copy(a, o, side).start()
+            push_copy(a, o, 1 + side).start()
+
+    def corners(k):
+        a, o = at(k)
+        for side in (1, 0):
+            relay_copy(a, o, side).wait_recv()
+            push_copy(a, o, 3 + side).start()
+
+    slots = lax.broadcasted_iota(jnp.int32, (capacity, tokens), 0).astype(jnp.float32)
+    slots = slots + (me * capacity).astype(jnp.float32)
+
+    def compact(k, source):
+        a = k % 2
+        info = metas[source]
+        hit0 = info[0:1, :] == slots
+        hit1 = info[1:2, :] == slots
+        place = jnp.where(hit0 | hit1, 1.0, 0.0).astype(jnp.bfloat16)
+        into = rows_of((rows_out, cot_out)[a], source, capacity)
+        if a == 1:
+            scale = jnp.where(hit0, info[2:3, :], 0.0) + jnp.where(hit1, info[3:4, :], 0.0)
+            scale = jnp.sum(scale, axis=1, keepdims=True)
+        for part in range(4):
+            span = pl.ds(part * width, width)
+            value = jnp.dot(
+                place, toks[a][source, :, span], preferred_element_type=jnp.float32
+            )
+            if a == 1:
+                value = value * scale
+            into[:, span] = value.astype(jnp.bfloat16)
+
+    def gather_rows(k):
+        a, o = at(k)
+        compact(k, 2 * o + lane)
+        for q in range(5):
+            push_copy(a, o, q, 1 - lane).wait_recv()
+        compact(k, 2 * o + 1 - lane)
+
+    pl.semaphore_wait(pltpu.get_barrier_semaphore(), count + 1)
     for a in range(2):
-        own_copy(a).start()
-    for target in others:
-        for a in range(2):
-            out_copy(a, target).start()
-    gather = ChipGather(mixed, mixed_out, mixed_sems, me, tp, count)
-    gather.start()
-
-    def relay_of(step):
-        return (across, down) if step % 2 == 0 else (down, across)
-
-    def relay(step):
-        source = (me + count - step) % count
-        owner, target = relay_of(step)
-        for a in range(2):
-            side_copy(a, source, owner, target, 3).wait_recv()
-            side_copy(a, source, owner, target, 3).start()
-
-    for step in range(count):
-        source = (me + count - step) % count
-        for a in range(2):
-            if step == 0:
-                own_copy(a).wait()
-            else:
-                side_copy(a, source, tp, across, 1).wait_recv()
-            side_copy(a, source, tp, across, 1).start()
-            side_copy(a, source, tp, down, 2).start()
-        if step >= 1:
-            relay(step - 1)
-    relay(count - 1)
-    gather.pass_on()
-    for step in range(count):
-        source = (me + count - step) % count
-        owner, target = relay_of(step)
-        for a in range(2):
-            side_copy(a, source, target, across, 1).wait_recv()
-            side_copy(a, source, corner, across, 1).wait_recv()
-            side_copy(a, source, tp, across, 1).wait_send()
-            side_copy(a, source, tp, down, 2).wait_send()
-            side_copy(a, source, owner, target, 3).wait_send()
-    for target in others:
-        for a in range(2):
-            out_copy(a, target).wait_send()
-    gather.finish()
-
-
-def dispatch(rows, cot, mixed, count):
-    capacity, width = rows.shape[1:]
-    full = jax.ShapeDtypeStruct((count * capacity, width * lax.axis_size("tp")), jnp.bfloat16)
+        z_start(a)
+        spread(a)
+    for other in others:
+        meta_copy(other).start()
+    ahead = 2
+    for n in range(blocks + 2):
+        if n == 0:
+            z_relay(*at(ahead))
+            ahead += 1
+        if n < blocks:
+            sides(n)
+        if n + 2 < blocks:
+            spread(n + 2)
+        while ahead < min(blocks, 4 + 2 * n if n < 2 else 5 + n):
+            z_relay(*at(ahead))
+            ahead += 1
+        if n == chips - 1:
+            z_start(2)
+            z_start(3)
+            pass_copy(2, z).start()
+            pass_copy(3, z).start()
+        if chips + 1 <= n < 2 * chips:
+            o = nearby(z, chips, n - chips)
+            for a in (2, 3):
+                z_relay(a, o)
+                pass_copy(a, o).start()
+        if n == 1:
+            for other in others:
+                remote(
+                    meta, metas.at[other], meta_send.at[other], meta_recv.at[other], other, tp
+                ).wait_recv()
+        if 1 <= n <= blocks:
+            corners(n - 1)
+        if 2 <= n:
+            gather_rows(n - 2)
+    for other in others:
+        meta_copy(other).wait_send()
+    for k in range(blocks):
+        a, o = at(k)
+        for side in range(2):
+            side_copy(a, o, side).wait_send()
+            relay_copy(a, o, side).wait_send()
+        for q in range(5):
+            push_copy(a, o, q).wait_send()
+    for a in range(4):
+        z_drain(a)
+        for j in range(1, chips):
+            z_finish(a, j)
+        if a >= 2:
+            for j in range(chips):
+                o = z if j == 0 else nearby(z, chips, j)
+                pass_copy(a, o, 1 - lane).wait_recv()
+                pass_copy(a, o).wait_send()
+
+
+def dispatch(x, cot, routes, weights, conv_out, row_mean, row_rstd, gain, proj, count):
+    tokens, width = x.shape
+    capacity = 4 * tokens // count
+    chips = count // 2
+    full = width * lax.axis_size("tp")
+    rows = jax.ShapeDtypeStruct((count * capacity, full), jnp.bfloat16)
+    dma = pltpu.SemaphoreType.DMA
     return pl.pallas_call(
         functools.partial(dispatch_kernel, count),
         out_shape=(
-            full,
-            full,
-            jax.ShapeDtypeStruct((count * mixed.shape[0], mixed.shape[1]), mixed.dtype),
+            rows,
+            rows,
+            jax.ShapeDtypeStruct((count * tokens, conv_out.shape[1]), jnp.bfloat16),
+            jax.ShapeDtypeStruct((count * proj.shape[0], proj.shape[1]), jnp.bfloat16),
+            jax.ShapeDtypeStruct((8, tokens), jnp.float32),
         ),
-        in_specs=[VMEM] * 3,
-        out_specs=(VMEM,) * 3,
+        in_specs=[pl.BlockSpec(memory_space=pltpu.HBM)] * 9,
+        out_specs=(VMEM,) * 5,
         scratch_shapes=[
-            pltpu.SemaphoreType.DMA((2, count, 4)),
-            pltpu.SemaphoreType.DMA((2, count, 4)),
-            pltpu.SemaphoreType.DMA((2,)),
+            pltpu.VMEM((count, tokens, full), jnp.bfloat16),
+            pltpu.VMEM((count, tokens, full), jnp.bfloat16),
+            pltpu.VMEM((count, 8, tokens), jnp.float32),
         ]
-        + gather_sems(count),
+        + [
+            pltpu.VMEM(value.shape, value.dtype)
+            for value in (routes, weights, conv_out, row_mean, row_rstd, gain)
+        ]
+        + [
+            dma((9,)),
+            dma((4, chips, 2)),
+            dma((4, chips)),
+            dma((2, chips, 2)),
+            dma((2, chips, 2)),
+            dma((2, chips, 2)),
+            dma((2, chips, 2)),
+            dma((4, chips, 5)),
+            dma((4, chips, 5)),
+            dma((count,)),
+            dma((count,)),
+        ],
         compiler_params=pltpu.CompilerParams(
-            collective_id=0, has_side_effects=True, vmem_limit_bytes=40 << 20
+            collective_id=0, has_side_effects=True, vmem_limit_bytes=36 << 20
         ),
         name="dispatch",
         cost_estimate=pl.CostEstimate(
-            flops=0, bytes_accessed=200 * rows.size * 2, transcendentals=0
+            flops=8 * count * capacity * tokens * full,
+            bytes_accessed=200 * count * capacity * width * 2,
+            transcendentals=0,
         ),
-    )(rows, cot, mixed)
+    )(*[pltpu.with_memory_space_constraint(v, pltpu.HBM) for v in (x, cot, routes, weights, conv_out, row_mean, row_rstd, gain, proj)])
 
 
 def combine_kernel(
     count,
     partial_ref,
     cot,
-    pick,
-    proj,
+    meta,
+    proj_all,
     conv_out,
     row_mean,
     row_rstd,
@@ -375,7 +582,6 @@
     reduced,
     back,
     stream,
-    proj_all,
     sums,
     arrived,
     extended,
@@ -392,7 +598,6 @@
     sum_recv,
     edge_send,
     edge_recv,
-    *proj_sems,
 ):
     me, tp = lax.axis_index("sp"), lax.axis_index("tp")
     capacity, width = reduced.shape[1:]
@@ -483,8 +688,9 @@
     window = min(WINDOW, count)
     for step in range(window):
         begin(step)
-    gather = ChipGather(proj, proj_all, proj_sems, me, tp, count)
-    gather.start()
+    slots = lax.broadcasted_iota(jnp.int32, (count * capacity, tokens), 0).astype(jnp.float32)
+    pick = jnp.where((meta[0:1, :] == slots) | (meta[1:2, :] == slots), 1.0, 0.0)
+    pick = pick.astype(jnp.bfloat16)
     rstd = jnp.broadcast_to(row_rstd[...], (tokens, tokens)).T[:, 0:1]
     mean = jnp.broadcast_to(row_mean[...], (tokens, tokens)).T[:, 0:1]
     normed = (conv_out[...].astype(jnp.float32) - mean) * rstd
@@ -499,7 +705,6 @@
         if step >= 1:
             settle(step - 1)
     settle(count - 1)
-    gather.pass_on()
     for other in others:
         remote(
             reduced.at[other],
@@ -509,7 +714,7 @@
             other,
             tp,
         ).wait_recv()
-    mine = jnp.dot(pick[...], back[...], preferred_element_type=jnp.float32)
+    mine = contract_rows(pick, back[...])
     mine_out[...] = mine
 
     def quarter(index):
@@ -523,7 +728,6 @@
 
     for q in range(3):
         wide_copy(q).start()
-    gather.finish()
 
     def part(index):
         return jnp.dot(
@@ -634,7 +838,7 @@
 
 
 def combine(
-    partial_value, cot, pick, proj, conv_out, row_mean, row_rstd, gain, taps, acts, count
+    partial_value, cot, meta, proj, conv_out, row_mean, row_rstd, gain, taps, acts, count
 ):
     tokens, width = cot.shape
     channels = conv_out.shape[1]
@@ -659,7 +863,6 @@
             pltpu.VMEM((count, capacity, width), jnp.bfloat16),
             pltpu.VMEM((count * capacity, width), jnp.bfloat16),
             pltpu.VMEM((tokens, full), jnp.bfloat16),
-            pltpu.VMEM((count * proj.shape[0], proj.shape[1]), jnp.bfloat16),
             pltpu.VMEM((8, tokens), jnp.float32),
             pltpu.VMEM((3, 8, tokens), jnp.float32),
             pltpu.VMEM((tokens + halo, channels), jnp.float32),
@@ -676,8 +879,7 @@
             dma((3,)),
             dma,
             dma,
-        ]
-        + gather_sems(count),
+        ],
         compiler_params=pltpu.CompilerParams(
             collective_id=1, has_side_effects=True, vmem_limit_bytes=24 << 20
         ),
@@ -687,7 +889,7 @@
             bytes_accessed=50 * partial_value.size * 2,
             transcendentals=0,
         ),
-    )(partial_value, cot, pick, proj, conv_out, row_mean, row_rstd, gain, taps, *acts)
+    )(partial_value, cot, meta, proj, conv_out, row_mean, row_rstd, gain, taps, *acts)
 
 
 def finish_kernel(
@@ -794,41 +996,16 @@
     out_proj,
 ):
     experts = lax.axis_size("sp")
-    tokens, width = moe_input.shape
-    capacity = 4 * tokens // experts
-    total = experts * capacity
-    flat_routes = routes.reshape(-1)
-    member = (flat_routes[:, None] == jnp.arange(experts, dtype=jnp.int32)[None, :]).astype(
-        jnp.bfloat16
-    )
-    index = jnp.arange(2 * tokens, dtype=jnp.int32)
-    before = (index[None, :] < index[:, None]).astype(jnp.bfloat16)
-    earlier = jnp.dot(before, member, preferred_element_type=jnp.float32)
-    slot_index = jnp.sum(earlier * member.astype(jnp.float32), axis=1).astype(jnp.int32)
-    buffer_row = (flat_routes * capacity + slot_index).reshape(tokens, 2)
-    places = jnp.arange(total, dtype=jnp.int32)
-    place0 = (buffer_row[:, 0][:, None] == places[None, :]).astype(jnp.bfloat16)
-    place1 = (buffer_row[:, 1][:, None] == places[None, :]).astype(jnp.bfloat16)
-    pick = place0 + place1
-    cot32 = cotangent.astype(jnp.float32)
-    weighted = jnp.concatenate(
-        [
-            (route_weight[:, 0:1] * cot32).astype(jnp.bfloat16),
-            (route_weight[:, 1:2] * cot32).astype(jnp.bfloat16),
-        ],
-        axis=0,
-    )
-    rows_buf = contract_rows(pick, moe_input).astype(jnp.bfloat16)
-    cot_buf = contract_rows(jnp.concatenate([place0, place1], axis=0), weighted).astype(
-        jnp.bfloat16
-    )
-    normed = (conv_out.astype(jnp.float32) - row_mean[:, None]) * row_rstd[:, None]
-    scaled_norm = normed * ln_gain[None, :]
-    mixed = (scaled_norm * jax.nn.sigmoid(scaled_norm)).astype(jnp.bfloat16)
-    expert_in, expert_cot, mixed_all = dispatch(
-        rows_buf.reshape(experts, capacity, width),
-        cot_buf.reshape(experts, capacity, width),
-        mixed,
+    expert_in, expert_cot, mixed_all, proj_all, meta = dispatch(
+        moe_input,
+        cotangent,
+        routes.T,
+        route_weight.T,
+        conv_out,
+        row_mean[None, :],
+        row_rstd[None, :],
+        ln_gain[None, :],
+        out_proj,
         experts,
     )
     gate_w = w_gate[0]
@@ -848,8 +1025,8 @@
     mine, unit_grad, columns, grads = combine(
         partial_value.astype(jnp.bfloat16),
         cotangent,
-        pick,
-        out_proj,
+        meta,
+        proj_all,
         conv_out,
         row_mean[None, :],
         row_rstd[None, :],

time: 120 us -> 109 us (0.908)
  Pallas kernels: 103 us -> 98.4 us
  other arithmetic: 3.12 us -> 0 us
  local copies, waits for them, and re-layouts: 2.26 us -> 0.18 us
    pallas_call x1, Pallas kernels: 57.2 us -> 49.6 us  [combine(): pl.pallas_call(functools.partial(combine_kernel, count), out_shape=(jax.S...]
    pallas_call x1, Pallas kernels: 41.6 us -> 45.1 us  [dispatch(): pl.pallas_call(functools.partial(dispatch_kernel, count), out_shape=(rows...]
    convert_element_type x4 -> x0, other arithmetic: 2.15 us -> none  [the longest x1 1.03 us: kernel_shards(): mixed = (scaled_norm * jax.nn.sigmoid(scaled_norm)).astype(jnp.bfloat16)]
    dot_general x4 -> x2, matrix products: 4.56 us -> 4 us  [contract_rows(): lax.dot_general(left, right, (((0,), (0,)), ((), ())), preferred_element_...]
where the time goes in v2:
time: 109 us
  Pallas kernels  98.4 us (90%)
  matrix products  9.69 us (9%)
    pallas_call x1, Pallas kernels, combine(): pl.pallas_call(functools.partial(combine_kernel, count), out_shape=(jax.S...  49.6 us
    pallas_call x1, Pallas kernels, dispatch(): pl.pallas_call(functools.partial(dispatch_kernel, count), out_shape=(rows...  45.1 us
    dot_general x3, matrix products, contract_cols(): lax.dot_general(left, right, (((1,), (1,)), ((), ())), preferred_element_...  5.69 us
    dot_general x2, matrix products, contract_rows(): lax.dot_general(left, right, (((0,), (0,)), ((), ())), preferred_element_...  4 us
    pallas_call x1, Pallas kernels, finish(): pl.pallas_call(finish_kernel, out_shape=tuple((jax.ShapeDtypeStruct(shape...  3.73 us

profile of v2, /device:TPU:9, one launch (start us, length us, event | category | flops | bytes accessed | tf_op | source)
XLA Modules:
  0.0 109.3 jit_solution(14396981006392769920)
XLA Ops:
  0.6 0.0 copy-start
  0.6 0.0 copy-start.10
  0.7 45.1 %dispatch.1 = (bf16[512,2048]{1,0:T(8,128)(2,1)S(1)}, bf16[512,2048]{1,0:T(8,128)(2,1)S(1)}, bf16[1024,256]{1,0:T(8,128)(2,1)S(1)}, bf16[2048,256]{1,0:T(8,128)(2,1)S(1)}, f32[8,128]{1,0:T(8,128)S(1)}) custom-call(bf16[128,512]{1,0:T(8,128)(2,1)} %x.1, bf16[128,512]{1,0:T(8,128)(2,1)} %cot.5, s32[2,128]{1,0:T(2,128)} %bitcast.43, f32[2,128]{1,0:T(2,128)} %bitcast.44, ...), custom_call_target="tpu_custom_call" | custom-call | flops 1073741824 | bytes 104857600 | tf_op jit(solution)/shard_map/dispatch/pallas_call | solution.py:515
  45.8 0.0 copy-done.10
  45.8 0.0 copy-start.9
  45.8 1.7 %fusion.9 = f32[704,512]{1,0:T(8,128)S(1)} fusion(bf16[512,2048]{1,0:T(8,128)(2,1)S(1)} %get-tuple-element.16.expert_cot, bf16[1,704,2048]{2,1,0:T(8,128)(2,1)S(1)} %copy-done.10), kind=kOutput, calls=%fused_computation.10 | convolution fusion | flops 1476395008 | bytes 6422528 | tf_op jit(solution)/shard_map/dot_general | solution.py:34
  47.5 0.1 copy-done.9
  47.6 1.8 %fusion.15 = f32[704,512]{1,0:T(8,128)S(1)} fusion(bf16[512,2048]{1,0:T(8,128)(2,1)S(1)} %get-tuple-element.17.expert_in, bf16[1,704,2048]{2,1,0:T(8,128)(2,1)S(1)} %copy-done.9), kind=kOutput, calls=%fused_computation.12 | convolution fusion | flops 1476395008 | bytes 6422528 | tf_op jit(solution)/shard_map/dot_general | solution.py:34
  49.3 0.0 copy-done
  49.4 2.3 %multiply_convert_fusion = (bf16[704,512]{1,0:T(8,128)(2,1)S(1)}, bf16[704,512]{1,0:T(8,128)(2,1)S(1)}, bf16[704,512]{1,0:T(8,128)(2,1)S(1)}) fusion(f32[704,512]{1,0:T(8,128)S(1)} %fusion.15, f32[704,512]{1,0:T(8,128)S(1)} %fusion.9, bf16[512,2048]{1,0:T(8,128)(2,1)S(1)} %get-tuple-element.17.expert_in, bf16[1,704,2048]{2,1,0:T(8,128)(2,1)S(1)} %copy-done), kind=kOutput, calls=%fused_computation.13 | convolution fusion | flops 1481801728 | bytes 10027008 | tf_op jit(solution)/shard_map/dot_general | solution.py:34
  51.6 1.9 %fusion = f32[512,2048]{1,0:T(8,128)S(1)} fusion(bf16[704,512]{1,0:T(8,128)(2,1)S(1)} %get-tuple-element.26.gate_delta, bf16[1,704,2048]{2,1,0:T(8,128)(2,1)S(1)} %copy-done.9), kind=kOutput, calls=%fused_computation.1 | convolution fusion | flops 1476395008 | bytes 7798784 | tf_op jit(solution)/shard_map/dot_general | solution.py:28
  53.5 0.0 copy-start.1
  53.5 0.0 copy-start.2
  53.5 0.0 copy-start.5
  53.5 0.0 copy-start.6
  53.5 0.0 copy-start.7
  53.5 0.0 copy-start.8
  53.6 2.1 %add_convert_fusion.partial_ref = bf16[512,2048]{1,0:T(8,128)(2,1)S(1)} fusion(f32[512,2048]{1,0:T(8,128)S(1)} %fusion, bf16[704,512]{1,0:T(8,128)(2,1)S(1)} %get-tuple-element.27.up_delta, bf16[1,704,2048]{2,1,0:T(8,128)(2,1)S(1)} %copy-done), kind=kOutput, calls=%fused_computation | convolution fusion | flops 1478492160 | bytes 9895936 | tf_op jit(solution)/shard_map/dot_general | solution.py:28
  55.7 0.0 copy-done.1
  55.7 0.0 copy-done.2
  55.7 0.0 copy-done.5
  55.7 0.0 copy-done.6
  55.7 0.0 copy-done.7
  55.8 0.0 copy-done.8
  55.8 0.0 copy-start.3
  55.8 0.0 copy-start.4
  55.8 49.6 %combine.1 = (f32[128,512]{1,0:T(8,128)S(1)}, f32[128,256]{1,0:T(8,128)S(1)}, bf16[1024,256]{1,0:T(8,128)(2,1)S(1)}, bf16[3,704,2048]{2,1,0:T(8,128)(2,1)S(1)}) custom-call(bf16[512,2048]{1,0:T(8,128)(2,1)S(1)} %add_convert_fusion.partial_ref, bf16[128,512]{1,0:T(8,128)(2,1)S(1)} %copy-done.1, f32[8,128]{1,0:T(8,128)S(1)} %get-tuple-element.18.meta, ...), custom_call_target="tpu_custom_call" | custom-call | flops 134217728 | bytes 104857600 | tf_op jit(solution)/shard_map/combine/pallas_call | solution.py:850
  105.3 0.0 copy-done.3
  105.4 0.0 copy-done.4
  105.4 3.7 %finish.1 = (bf16[1,704,2048]{2,1,0:T(8,128)(2,1)}, bf16[1,704,2048]{2,1,0:T(8,128)(2,1)}, bf16[1,704,2048]{2,1,0:T(8,128)(2,1)}, f32[256,256]{1,0:T(8,128)}, bf...) custom-call(bf16[3,704,2048]{2,1,0:T(8,128)(2,1)S(1)} %get-tuple-element.20.grads, ...), custom_call_target="tpu_custom_call" | custom-call | flops 134217728 | bytes 17301504 | tf_op jit(solution)/shard_map/finish/pallas_call | solution.py:953
Async XLA Ops:
  0.6 48.7 %copy-start = (bf16[1,704,2048]{2,1,0:T(8,128)(2,1)S(1)}, bf16[1,704,2048]{2,1,0:T(8,128)(2,1)}, u32[]{:S(2)}) copy-start(bf16[1,704,2048]{2,1,0:T(8,128)(2,1)} %param.20) | copy-start | bytes 8650756
  0.6 45.1 %copy-start.10 = (bf16[1,704,2048]{2,1,0:T(8,128)(2,1)S(1)}, bf16[1,704,2048]{2,1,0:T(8,128)(2,1)}, u32[]{:S(2)}) copy-start(bf16[1,704,2048]{2,1,0:T(8,128)(2,1)} %param.21) | copy-start | bytes 8650756
  45.8 1.8 %copy-start.9 = (bf16[1,704,2048]{2,1,0:T(8,128)(2,1)S(1)}, bf16[1,704,2048]{2,1,0:T(8,128)(2,1)}, u32[]{:S(2)}) copy-start(bf16[1,704,2048]{2,1,0:T(8,128)(2,1)} %param.19) | copy-start | bytes 8650756
  53.5 2.2 %copy-start.1 = (bf16[128,512]{1,0:T(8,128)(2,1)S(1)}, bf16[128,512]{1,0:T(8,128)(2,1)}, u32[]{:S(2)}) copy-start(bf16[128,512]{1,0:T(8,128)(2,1)} %cot.5) | copy-start | bytes 393220
  53.5 2.2 %copy-start.2 = (bf16[128,256]{1,0:T(8,128)(2,1)S(1)}, bf16[128,256]{1,0:T(8,128)(2,1)}, u32[]{:S(2)}) copy-start(bf16[128,256]{1,0:T(8,128)(2,1)} %conv_out.1) | copy-start | bytes 196612
  53.5 2.2 %copy-start.5 = (bf16[31,256]{1,0:T(8,128)(2,1)S(1)}, bf16[31,256]{1,0:T(8,128)(2,1)}, u32[]{:S(2)}) copy-start(bf16[31,256]{1,0:T(8,128)(2,1)} %taps.1) | copy-start | bytes 47620
  53.5 2.2 %copy-start.6 = (f32[256]{0:T(256)S(1)}, f32[256]{0:T(256)}, u32[]{:S(2)}) copy-start(f32[256]{0:T(256)} %param.27) | copy-start | bytes 3076
  53.5 2.2 %copy-start.7 = (f32[128]{0:T(128)S(1)}, f32[128]{0:T(128)}, u32[]{:S(2)}) copy-start(f32[128]{0:T(128)} %param.25) | copy-start | bytes 1540
  53.5 2.2 %copy-start.8 = (f32[128]{0:T(128)S(1)}, f32[128]{0:T(128)}, u32[]{:S(2)}) copy-start(f32[128]{0:T(128)} %param.26) | copy-start | bytes 1540
  55.8 49.6 %copy-start.3 = (bf16[128,256]{1,0:T(8,128)(2,1)S(1)}, bf16[128,256]{1,0:T(8,128)(2,1)}, u32[]{:S(2)}) copy-start(bf16[128,256]{1,0:T(8,128)(2,1)} %v_value.1) | copy-start | bytes 196612
  55.8 49.6 %copy-start.4 = (bf16[128,256]{1,0:T(8,128)(2,1)S(1)}, bf16[128,256]{1,0:T(8,128)(2,1)}, u32[]{:S(2)}) copy-start(bf16[128,256]{1,0:T(8,128)(2,1)} %v_gate.1) | copy-start | bytes 196612

commit v3 on v2

--- a/solution.py
+++ b/solution.py
@@ -169,15 +169,6 @@
     )
 
 
-def greet(peers):
-    barrier = pltpu.get_barrier_semaphore()
-    for sp, tp in peers:
-        pl.semaphore_signal(
-            barrier, inc=1, device_id={"sp": sp, "tp": tp}, device_id_type=pl.DeviceIdType.MESH
-        )
-    pl.semaphore_wait(barrier, len(peers))
-
-
 def rows_of(ref, index, count):
     return ref.at[pl.ds(pl.multiple_of(index * count, count), count)]
 
@@ -200,7 +191,7 @@
     return both * two + (1 - both) * one
 
 
-def dispatch_kernel(
+def whole_kernel(
     count,
     x,
     cot,
@@ -211,20 +202,47 @@
     rstd_far,
     gain_far,
     proj,
-    rows_out,
-    cot_out,
+    taps_far,
+    gate_far,
+    up_far,
+    down_far,
+    mine_out,
+    unit_out,
+    strips,
     mixed_all,
-    proj_all,
-    meta,
+    grads,
     tok_x,
     tok_c,
     metas,
+    meta,
+    proj_all,
     routes,
     weights,
     conv_out,
     row_mean,
     row_rstd,
     gain,
+    taps,
+    gate_w,
+    up_w,
+    down_w,
+    rows,
+    cots,
+    hidden,
+    gate_delta,
+    up_delta,
+    first_factor,
+    second_factor,
+    turned,
+    partial_ref,
+    landed,
+    middle,
+    reduced,
+    back,
+    stream,
+    sums,
+    arrived,
+    extended,
     load,
     z_send,
     z_recv,
@@ -236,16 +254,33 @@
     push_recv,
     meta_send,
     meta_recv,
+    send,
+    recv,
+    back_send,
+    back_recv,
+    wide_send,
+    wide_recv,
+    strip_send,
+    strip_recv,
+    sum_send,
+    sum_recv,
+    part_send,
+    part_recv,
+    edge_send,
+    edge_recv,
 ):
     me, tp = lax.axis_index("sp"), lax.axis_index("tp")
     tokens, width = x.shape
-    capacity = rows_out.shape[0] // count
+    capacity = rows.shape[0] // count
+    units = hidden.shape[0]
+    channels = conv_out.shape[1]
     chips = count // 2
     z, lane = me // 2, me % 2
     partner = me + 1 - 2 * lane
     across, down, corner = tp + 1 - 2 * (tp % 2), (tp + 2) % 4, 3 - tp
     others = [(me + d) % count for d in range(1, count)]
-    announce([(other, tp) for other in others] + [(me, across), (me, down)])
+    group = (across, down, corner)
+    announce([(other, tp) for other in others] + [(me, other) for other in group])
     half = tokens // 2
     toks = (tok_x, tok_c)
     gathered = (mixed_all, proj_all)
@@ -269,12 +304,16 @@
                 (rstd_far, row_rstd),
                 (gain_far, gain),
                 (proj, rows_of(proj_all, me, proj.shape[0])),
+                (taps_far, taps),
+                (gate_far.at[0], gate_w),
+                (up_far.at[0], up_w),
+                (down_far.at[0], down_w),
             )
         )
     ]
     for copy in loads:
         copy.start()
-    for copy in loads:
+    for copy in loads[:-3]:
         copy.wait()
     rstd = jnp.broadcast_to(row_rstd[...], (tokens, tokens)).T[:, 0:1]
     mean = jnp.broadcast_to(row_mean[...], (tokens, tokens)).T[:, 0:1]
@@ -394,11 +433,17 @@
             meta, metas.at[me], meta_send.at[target], meta_recv.at[me], target, tp
         )
 
+    early = list(range(chips // 2))
+    late = list(range(chips // 2, chips))
+    line = [(a, j) for j in early for a in range(2)] + [(a, j) for a in range(2) for j in late]
+    blocks = len(line)
+
+    def plane(j):
+        return z if j == 0 else nearby(z, chips, j)
+
     def at(k):
-        j, a = k // 2, k % 2
-        return a, (z if j == 0 else nearby(z, chips, j))
-
-    blocks = 2 * chips
+        a, j = line[k]
+        return a, plane(j)
 
     def spread(k):
         a, o = at(k)
@@ -422,13 +467,12 @@
     slots = lax.broadcasted_iota(jnp.int32, (capacity, tokens), 0).astype(jnp.float32)
     slots = slots + (me * capacity).astype(jnp.float32)
 
-    def compact(k, source):
-        a = k % 2
+    def compact(a, source, place_at):
         info = metas[source]
         hit0 = info[0:1, :] == slots
         hit1 = info[1:2, :] == slots
         place = jnp.where(hit0 | hit1, 1.0, 0.0).astype(jnp.bfloat16)
-        into = rows_of((rows_out, cot_out)[a], source, capacity)
+        into = (rows, cots)[a].at[pl.ds(place_at * capacity, capacity)]
         if a == 1:
             scale = jnp.where(hit0, info[2:3, :], 0.0) + jnp.where(hit1, info[3:4, :], 0.0)
             scale = jnp.sum(scale, axis=1, keepdims=True)
@@ -443,12 +487,142 @@
 
     def gather_rows(k):
         a, o = at(k)
-        compact(k, 2 * o + lane)
+        j = line[k][1]
+        compact(a, 2 * o + lane, 2 * j)
         for q in range(5):
             push_copy(a, o, q, 1 - lane).wait_recv()
-        compact(k, 2 * o + 1 - lane)
-
-    pl.semaphore_wait(pltpu.get_barrier_semaphore(), count + 1)
+        compact(a, 2 * o + 1 - lane, 2 * j + 1)
+
+    batch = rows.shape[0] // 2
+    tiles = 1
+    tile = units // tiles
+    breadth = 512 if width % 512 == 0 else width
+    pieces = 4 * width // breadth
+
+    def activate(h):
+        span = pl.ds(h * batch, batch)
+
+        def step(t, carry):
+            u = pl.ds(pl.multiple_of(t * tile, 16), tile)
+            gate = contract_cols(gate_w[u, :], rows[span, :])
+            up = contract_cols(up_w[u, :], rows[span, :])
+            gate_sig = jax.nn.sigmoid(gate)
+            gate_act = gate * gate_sig
+            hidden[u, span] = (gate_act * up).astype(jnp.bfloat16)
+            first_factor[u, :] = up * gate_sig * (1.0 + gate * (1.0 - gate_sig))
+            second_factor[u, :] = gate_act
+            return carry
+
+        lax.fori_loop(0, tiles, step, 0)
+
+    def deltas(h):
+        span = pl.ds(h * batch, batch)
+
+        def step(t, carry):
+            u = pl.ds(pl.multiple_of(t * tile, 16), tile)
+            hidden_grad = contract_cols(down_w[u, :], cots[span, :])
+            gate_delta[u, span] = (hidden_grad * first_factor[u, :]).astype(jnp.bfloat16)
+            up_delta[u, span] = (hidden_grad * second_factor[u, :]).astype(jnp.bfloat16)
+            return carry
+
+        lax.fori_loop(0, tiles, step, 0)
+        turned[0] = gate_delta[:, span].T
+        turned[1] = up_delta[:, span].T
+
+    def partials(h, first_piece, last_piece):
+        span = pl.ds(h * batch, batch)
+
+        def step(t, carry):
+            spots = pl.ds(pl.multiple_of(t * breadth, 128), breadth)
+            value = jnp.dot(turned[0], gate_w[:, spots], preferred_element_type=jnp.float32)
+            value = value + jnp.dot(
+                turned[1], up_w[:, spots], preferred_element_type=jnp.float32
+            )
+            partial_ref[span, spots] = value.astype(jnp.bfloat16)
+            return carry
+
+        lax.fori_loop(first_piece, last_piece, step, 0)
+
+    products = ((gate_delta, rows), (up_delta, rows), (hidden, cots))
+
+    def product(spot, carry):
+        spots = pl.ds(pl.multiple_of(spot * breadth, 128), breadth)
+        for a, (left, right) in enumerate(products):
+            value = jnp.dot(left[...], right[:, spots], preferred_element_type=jnp.float32)
+            grads[a, :, spots] = value.astype(jnp.bfloat16)
+        return carry
+
+    def share(step, owner):
+        return partial_ref.at[
+            pl.ds(step * capacity, capacity),
+            pl.ds(pl.multiple_of(owner * width, 128), width),
+        ]
+
+    def source_of(step):
+        return 2 * plane(step // 2) + (lane if step % 2 == 0 else 1 - lane)
+
+    def near_far(step):
+        return (across, down) if step % 2 == 0 else (down, across)
+
+    def share_copy(step, q):
+        near = near_far(step)[0]
+        return remote(
+            share(step, corner if q == 1 else near),
+            landed.at[q, step],
+            send.at[step, q],
+            recv.at[step, q],
+            me,
+            near,
+        )
+
+    def middle_copy(step):
+        return remote(
+            middle.at[step],
+            landed.at[2, step],
+            send.at[step, 2],
+            recv.at[step, 2],
+            me,
+            near_far(step)[1],
+        )
+
+    def back_copy(step):
+        target = source_of(step)
+        return remote(
+            reduced.at[step],
+            rows_of(back, me, capacity),
+            back_send.at[step],
+            back_recv.at[me],
+            target,
+            tp,
+        )
+
+    def begin(steps):
+        for q in (1, 0):
+            for step in steps:
+                share_copy(step, q).start()
+
+    half_count = count // 2
+    lower, upper = range(half_count), range(half_count, count)
+
+    def forward(step):
+        share_copy(step, 1).wait_recv()
+        own = share(step, near_far(step)[1])[...].astype(jnp.float32)
+        middle[step] = (own + landed[1, step].astype(jnp.float32)).astype(jnp.bfloat16)
+        middle_copy(step).start()
+
+    def settle(step):
+        share_copy(step, 0).wait_recv()
+        middle_copy(step).wait_recv()
+        total = share(step, tp)[...].astype(jnp.float32)
+        total = total + landed[0, step].astype(jnp.float32)
+        total = (total + landed[2, step].astype(jnp.float32)).astype(jnp.bfloat16)
+        if step > 0:
+            reduced[step] = total
+            back_copy(step).start()
+        else:
+            back[pl.ds(pl.multiple_of(me * capacity, capacity), capacity), :] = total
+
+    pl.semaphore_wait(pltpu.get_barrier_semaphore(), count + 2)
     for a in range(2):
         z_start(a)
         spread(a)
@@ -463,7 +637,7 @@
             sides(n)
         if n + 2 < blocks:
             spread(n + 2)
-        while ahead < min(blocks, 4 + 2 * n if n < 2 else 5 + n):
+        while ahead < min(blocks, 4 if n == 0 else 3 + 2 * n):
             z_relay(*at(ahead))
             ahead += 1
         if n == chips - 1:
@@ -485,6 +659,46 @@
             corners(n - 1)
         if 2 <= n:
             gather_rows(n - 2)
+        if n == chips:
+            for copy in loads[-3:]:
+                copy.wait()
+            activate(0)
+        if n == chips + 1:
+            deltas(0)
+        if n == chips + 2:
+            partials(0, 0, pieces)
+        if n == chips + chips // 2 + 1:
+            activate(1)
+        if n == blocks - 1:
+            begin(lower)
+        if n == blocks:
+            forward(0)
+    slots_all = lax.broadcasted_iota(jnp.int32, (count * capacity, tokens), 0)
+    slots_all = slots_all.astype(jnp.float32)
+    deltas(1)
+    for step in lower[1:]:
+        partials(1, pieces * (step - 1) // (half_count - 1), pieces * step // (half_count - 1))
+        if step == half_count - 1:
+            begin(upper)
+        forward(step)
+        settle(step - 1)
+    lax.fori_loop(0, pieces // 4, product, 0)
+    settle(half_count - 1)
+    for step in upper:
+        forward(step)
+        if step == half_count + 1:
+            lax.fori_loop(pieces // 4, pieces // 2, product, 0)
+    pick = jnp.where((meta[0:1, :] == slots_all) | (meta[1:2, :] == slots_all), 1.0, 0.0)
+    pick = pick.astype(jnp.bfloat16)
+    rstd = jnp.broadcast_to(row_rstd[...], (tokens, tokens)).T[:, 0:1]
+    mean = jnp.broadcast_to(row_mean[...], (tokens, tokens)).T[:, 0:1]
+    normed = (conv_out[...].astype(jnp.float32) - mean) * rstd
+    scaled = normed * gain[...]
+    sig = jax.nn.sigmoid(scaled)
+    slope = sig * (1.0 + scaled * (1.0 - sig)) * gain[...]
+    for step in upper:
+        settle(step)
+    lax.fori_loop(pieces // 2, 3 * pieces // 4, product, 0)
     for other in others:
         meta_copy(other).wait_send()
     for k in range(blocks):
@@ -503,213 +717,11 @@
                 o = z if j == 0 else nearby(z, chips, j)
                 pass_copy(a, o, 1 - lane).wait_recv()
                 pass_copy(a, o).wait_send()
-
-
-def dispatch(x, cot, routes, weights, conv_out, row_mean, row_rstd, gain, proj, count):
-    tokens, width = x.shape
-    capacity = 4 * tokens // count
-    chips = count // 2
-    full = width * lax.axis_size("tp")
-    rows = jax.ShapeDtypeStruct((count * capacity, full), jnp.bfloat16)
-    dma = pltpu.SemaphoreType.DMA
-    return pl.pallas_call(
-        functools.partial(dispatch_kernel, count),
-        out_shape=(
-            rows,
-            rows,
-            jax.ShapeDtypeStruct((count * tokens, conv_out.shape[1]), jnp.bfloat16),
-            jax.ShapeDtypeStruct((count * proj.shape[0], proj.shape[1]), jnp.bfloat16),
-            jax.ShapeDtypeStruct((8, tokens), jnp.float32),
-        ),
-        in_specs=[pl.BlockSpec(memory_space=pltpu.HBM)] * 9,
-        out_specs=(VMEM,) * 5,
-        scratch_shapes=[
-            pltpu.VMEM((count, tokens, full), jnp.bfloat16),
-            pltpu.VMEM((count, tokens, full), jnp.bfloat16),
-            pltpu.VMEM((count, 8, tokens), jnp.float32),
-        ]
-        + [
-            pltpu.VMEM(value.shape, value.dtype)
-            for value in (routes, weights, conv_out, row_mean, row_rstd, gain)
-        ]
-        + [
-            dma((9,)),
-            dma((4, chips, 2)),
-            dma((4, chips)),
-            dma((2, chips, 2)),
-            dma((2, chips, 2)),
-            dma((2, chips, 2)),
-            dma((2, chips, 2)),
-            dma((4, chips, 5)),
-            dma((4, chips, 5)),
-            dma((count,)),
-            dma((count,)),
-        ],
-        compiler_params=pltpu.CompilerParams(
-            collective_id=0, has_side_effects=True, vmem_limit_bytes=36 << 20
-        ),
-        name="dispatch",
-        cost_estimate=pl.CostEstimate(
-            flops=8 * count * capacity * tokens * full,
-            bytes_accessed=200 * count * capacity * width * 2,
-            transcendentals=0,
-        ),
-    )(*[pltpu.with_memory_space_constraint(v, pltpu.HBM) for v in (x, cot, routes, weights, conv_out, row_mean, row_rstd, gain, proj)])
-
-
-def combine_kernel(
-    count,
-    partial_ref,
-    cot,
-    meta,
-    proj_all,
-    conv_out,
-    row_mean,
-    row_rstd,
-    gain,
-    taps,
-    hidden,
-    gate_delta,
-    up_delta,
-    expert_in,
-    expert_cot,
-    mine_out,
-    unit_out,
-    columns,
-    grads,
-    landed,
-    middle,
-    reduced,
-    back,
-    stream,
-    sums,
-    arrived,
-    extended,
-    send,
-    recv,
-    back_send,
-    back_recv,
-    wide_send,
-    wide_recv,
-    strip_send,
-    strip_recv,
-    strip_local,
-    sum_send,
-    sum_recv,
-    edge_send,
-    edge_recv,
-):
-    me, tp = lax.axis_index("sp"), lax.axis_index("tp")
-    capacity, width = reduced.shape[1:]
-    tokens, channels = conv_out.shape
-    across, down, corner = tp + 1 - 2 * (tp % 2), (tp + 2) % 4, 3 - tp
-    group = (across, down, corner)
-    others = [(me + d) % count for d in range(1, count)]
-    greet([(other, tp) for other in others] + [(me, other) for other in group])
-
-    def share(source, owner):
-        return partial_ref.at[
-            pl.ds(pl.multiple_of(source * capacity, capacity), capacity),
-            pl.ds(pl.multiple_of(owner * width, 128), width),
-        ]
-
-    order = others + [me]
-
-    def sides(step):
-        return (across, down) if step % 2 == 0 else (down, across)
-
-    def share_copy(step, q):
-        source, near = order[step], sides(step)[0]
-        return remote(
-            share(source, corner if q == 1 else near),
-            landed.at[q, source],
-            send.at[source, q],
-            recv.at[source, q],
-            me,
-            near,
-        )
-
-    def middle_copy(step):
-        source = order[step]
-        return remote(
-            middle.at[source],
-            landed.at[2, source],
-            send.at[source, 2],
-            recv.at[source, 2],
-            me,
-            sides(step)[1],
-        )
-
-    def back_copy(target):
-        return remote(
-            reduced.at[target],
-            rows_of(back, me, capacity),
-            back_send.at[target],
-            back_recv.at[me],
-            target,
-            tp,
-        )
-
-    def begin(step):
-        for q in (1, 0):
-            share_copy(step, q).start()
-
-    def forward(step):
-        source = order[step]
-        share_copy(step, 1).wait_recv()
-        own = share(source, sides(step)[1])[...].astype(jnp.float32)
-        middle[source] = (own + landed[1, source].astype(jnp.float32)).astype(jnp.bfloat16)
-        middle_copy(step).start()
-
-    def settle(step):
-        source = order[step]
-        share_copy(step, 0).wait_recv()
-        middle_copy(step).wait_recv()
-        total = share(source, tp)[...].astype(jnp.float32)
-        total = total + landed[0, source].astype(jnp.float32)
-        total = (total + landed[2, source].astype(jnp.float32)).astype(jnp.bfloat16)
-        if step < count - 1:
-            reduced[source] = total
-            back_copy(source).start()
-        else:
-            back[pl.ds(pl.multiple_of(me * capacity, capacity), capacity), :] = total
-
-    products = ((gate_delta, expert_in), (up_delta, expert_in), (hidden, expert_cot))
-    piece = PIECE if width % PIECE == 0 else width
-
-    def product(spot, carry):
-        spots = pl.ds(pl.multiple_of(spot * piece, 128), piece)
-        for a, (left, right) in enumerate(products):
-            value = jnp.dot(left[...], right[:, spots], preferred_element_type=jnp.float32)
-            grads[a, :, spots] = value.astype(jnp.bfloat16)
-        return carry
-
-    pieces = 4 * width // piece
-    window = min(WINDOW, count)
-    for step in range(window):
-        begin(step)
-    slots = lax.broadcasted_iota(jnp.int32, (count * capacity, tokens), 0).astype(jnp.float32)
-    pick = jnp.where((meta[0:1, :] == slots) | (meta[1:2, :] == slots), 1.0, 0.0)
-    pick = pick.astype(jnp.bfloat16)
-    rstd = jnp.broadcast_to(row_rstd[...], (tokens, tokens)).T[:, 0:1]
-    mean = jnp.broadcast_to(row_mean[...], (tokens, tokens)).T[:, 0:1]
-    normed = (conv_out[...].astype(jnp.float32) - mean) * rstd
-    scaled = normed * gain[...]
-    sig = jax.nn.sigmoid(scaled)
-    slope = sig * (1.0 + scaled * (1.0 - sig)) * gain[...]
-    for step in range(count):
-        lax.fori_loop(pieces * step // count, pieces * (step + 1) // count, product, 0)
-        forward(step)
-        if step + window < count:
-            begin(step + window)
-        if step >= 1:
-            settle(step - 1)
-    settle(count - 1)
     for other in others:
         remote(
-            reduced.at[other],
+            reduced.at[0],
             rows_of(back, other, capacity),
-            back_send.at[other],
+            back_send.at[0],
             back_recv.at[other],
             other,
             tp,
@@ -720,7 +732,7 @@
     def quarter(index):
         return pl.ds(pl.multiple_of(index * width, 128), width)
 
-    stream[:, quarter(tp)] = (cot[...].astype(jnp.float32) + mine).astype(jnp.bfloat16)
+    stream[:, quarter(tp)] = (block(1, me, tp)[...].astype(jnp.float32) + mine).astype(jnp.bfloat16)
 
     def wide_copy(q):
         spot = stream.at[:, quarter(tp)]
@@ -728,34 +740,57 @@
 
     for q in range(3):
         wide_copy(q).start()
-
-    def part(index):
+    lax.fori_loop(3 * pieces // 4, pieces, product, 0)
+
+    def share_of(index):
         return jnp.dot(
             stream[:, quarter(index)],
             proj_all[quarter(index), :],
             preferred_element_type=jnp.float32,
         )
 
-    mixed_grad = part(tp)
-    for q in range(3):
-        spot = stream.at[:, quarter(group[q])]
-        remote(spot, spot, wide_send.at[q], wide_recv.at[q], me, group[q]).wait_recv()
-        mixed_grad = mixed_grad + part(group[q])
     depth = stream.shape[1] // count
-
-    def strip(index):
-        return stream.at[:, pl.ds(pl.multiple_of(index * depth, 128), depth)]
+    part_rows = tokens // 4
+    part_strips = count // 4
+
+    def part_of(source, owner):
+        start = pl.multiple_of(source * tokens + owner * part_rows, part_rows)
+        return strips.at[pl.ds(start, part_rows)]
 
     def strip_copy(target):
         return remote(
-            strip(target),
-            rows_of(columns, me, tokens),
+            stream.at[
+                pl.ds(pl.multiple_of(tp * part_rows, part_rows), part_rows),
+                pl.ds(pl.multiple_of(target * depth, 128), depth),
+            ],
+            part_of(me, tp),
             strip_send.at[target],
             strip_recv.at[me],
             target,
             tp,
         )
 
+    def part_copy(source, q):
+        spot = part_of(source, tp)
+        return remote(
+            spot, spot, part_send.at[source, q], part_recv.at[source, q], me, group[q]
+        )
+
+    def strip_out(owner):
+        for index in range(part_strips):
+            target = owner * part_strips + index
+
+            @pl.when(target != me)
+            def _(target=target):
+                strip_copy(target).start()
+
+    strip_out(tp)
+    mixed_grad = share_of(tp)
+    for q in range(3):
+        spot = stream.at[:, quarter(group[q])]
+        remote(spot, spot, wide_send.at[q], wide_recv.at[q], me, group[q]).wait_recv()
+        strip_out(group[q])
+        mixed_grad = mixed_grad + share_of(group[q])
     norm_grad = mixed_grad * slope
     first = jnp.sum(norm_grad, axis=1, keepdims=True)
     second = jnp.sum(norm_grad * normed, axis=1, keepdims=True)
@@ -768,10 +803,8 @@
 
     for q in range(3):
         sum_copy(q).start()
-    own = pltpu.make_async_copy(strip(me), rows_of(columns, me, tokens), strip_local)
-    own.start()
-    for other in others:
-        strip_copy(other).start()
+    own_strip = stream[:, pl.ds(pl.multiple_of(me * depth, 128), depth)]
+    rows_of(strips, me, tokens)[...] = own_strip
     for q in range(3):
         sum_copy(q).wait()
     total = sums[...] + arrived[0] + arrived[1] + arrived[2]
@@ -797,35 +830,46 @@
     def _():
         extended[tokens:] = jnp.zeros((halo, channels), jnp.float32)
 
-    @pl.when(me < count - 1)
-    def _():
-        edge.wait_recv()
-
     kernel = taps.shape[0]
-    unit_grad = jnp.zeros((tokens, channels), jnp.float32)
-    for offset in range(kernel):
-        lead = kernel - 1 - offset
-        tap = taps[offset : offset + 1, :].astype(jnp.float32)
-        unit_grad = unit_grad + tap * extended[lead : lead + tokens, :]
-    unit_out[...] = unit_grad
-    own.wait()
+
+    def convolve(start, size):
+        unit_grad = jnp.zeros((size, channels), jnp.float32)
+        for offset in range(kernel):
+            lead = start + kernel - 1 - offset
+            tap = taps[offset : offset + 1, :].astype(jnp.float32)
+            unit_grad = unit_grad + tap * extended[lead : lead + size, :]
+        unit_out[start : start + size] = unit_grad
+
     for other in others:
         remote(
-            strip(other),
-            rows_of(columns, other, tokens),
+            part_of(other, tp),
+            part_of(other, tp),
             strip_send.at[other],
             strip_recv.at[other],
             other,
             tp,
         ).wait_recv()
+        for q in range(3):
+            part_copy(other, q).start()
+    convolve(0, tokens - halo)
+
+    @pl.when(me < count - 1)
+    def _():
+        edge.wait_recv()
+
+    convolve(tokens - halo, halo)
+    for other in others:
+        for q in range(3):
+            part_copy(other, q).wait()
     for q in range(3):
         wide_copy(q).wait_send()
     for step in range(count):
         share_copy(step, 0).wait_send()
         share_copy(step, 1).wait_send()
         middle_copy(step).wait_send()
+    for step in range(1, count):
+        back_copy(step).wait_send()
     for other in others:
-        back_copy(other).wait_send()
         strip_copy(other).wait_send()
 
     @pl.when(me > 0)
@@ -833,63 +877,85 @@
         edge.wait_send()
 
 
-WINDOW = 3
-PIECE = 256
-
-
-def combine(
-    partial_value, cot, meta, proj, conv_out, row_mean, row_rstd, gain, taps, acts, count
-):
-    tokens, width = cot.shape
+def whole(x, cot, routes, weights, conv_out, row_mean, row_rstd, gain, proj, taps, gate, up, down, count):
+    tokens, width = x.shape
     channels = conv_out.shape[1]
-    capacity = partial_value.shape[0] // count
-    full = partial_value.shape[1]
+    capacity = 4 * tokens // count
+    total = count * capacity
+    chips = count // 2
+    full = width * lax.axis_size("tp")
     depth = full // count
+    units = gate.shape[1]
     halo = -(-(taps.shape[0] - 1) // 8) * 8
+    bf16, f32 = jnp.bfloat16, jnp.float32
     dma = pltpu.SemaphoreType.DMA
+    operands = (x, cot, routes, weights, conv_out, row_mean, row_rstd, gain, proj, taps, gate, up, down)
+    vmem = [
+        ((count, tokens, full), bf16),
+        ((count, tokens, full), bf16),
+        ((count, 8, tokens), f32),
+        ((8, tokens), f32),
+        ((count * proj.shape[0], proj.shape[1]), bf16),
+    ]
+    vmem += [
+        (value.shape, value.dtype)
+        for value in (routes, weights, conv_out, row_mean, row_rstd, gain, taps)
+    ]
+    vmem += [
+        ((units, full), bf16),
+        ((units, full), bf16),
+        ((units, full), bf16),
+        ((total, full), bf16),
+        ((total, full), bf16),
+        ((units, total), bf16),
+        ((units, total), bf16),
+        ((units, total), bf16),
+        ((units, total // 2), f32),
+        ((units, total // 2), f32),
+        ((2, total // 2, units), bf16),
+        ((total, full), bf16),
+        ((3, count, capacity, width), bf16),
+        ((count, capacity, width), bf16),
+        ((count, capacity, width), bf16),
+        ((total, width), bf16),
+        ((tokens, full), bf16),
+        ((8, tokens), f32),
+        ((3, 8, tokens), f32),
+        ((tokens + halo, channels), f32),
+    ]
+    sems = [(len(operands),), (4, chips, 2), (4, chips)]
+    sems += [(2, chips, 2)] * 4
+    sems += [(4, chips, 5)] * 2
+    sems += [(count,)] * 2
+    sems += [(count, 3)] * 2
+    sems += [(count,)] * 2 + [(3,)] * 2 + [(count,)] * 2 + [(3,)] * 2 + [(count, 3)] * 2
     return pl.pallas_call(
-        functools.partial(combine_kernel, count),
+        functools.partial(whole_kernel, count),
         out_shape=(
-            jax.ShapeDtypeStruct((tokens, width), jnp.float32),
-            jax.ShapeDtypeStruct((tokens, channels), jnp.float32),
-            jax.ShapeDtypeStruct((count * tokens, depth), jnp.bfloat16),
-            jax.ShapeDtypeStruct((3, acts[0].shape[0], full), jnp.bfloat16),
+            jax.ShapeDtypeStruct((tokens, width), f32),
+            jax.ShapeDtypeStruct((tokens, channels), f32),
+            jax.ShapeDtypeStruct((count * tokens, depth), bf16),
+            jax.ShapeDtypeStruct((count * tokens, channels), bf16),
+            jax.ShapeDtypeStruct((3, units, full), bf16),
         ),
-        in_specs=[VMEM] * 14,
-        out_specs=(VMEM,) * 4,
-        scratch_shapes=[
-            pltpu.VMEM((3, count, capacity, width), jnp.bfloat16),
-            pltpu.VMEM((count, capacity, width), jnp.bfloat16),
-            pltpu.VMEM((count, capacity, width), jnp.bfloat16),
-            pltpu.VMEM((count * capacity, width), jnp.bfloat16),
-            pltpu.VMEM((tokens, full), jnp.bfloat16),
-            pltpu.VMEM((8, tokens), jnp.float32),
-            pltpu.VMEM((3, 8, tokens), jnp.float32),
-            pltpu.VMEM((tokens + halo, channels), jnp.float32),
-            dma((count, 3)),
-            dma((count, 3)),
-            dma((count,)),
-            dma((count,)),
-            dma((3,)),
-            dma((3,)),
-            dma((count,)),
-            dma((count,)),
-            dma,
-            dma((3,)),
-            dma((3,)),
-            dma,
-            dma,
-        ],
+        in_specs=[pl.BlockSpec(memory_space=pltpu.HBM)] * len(operands),
+        out_specs=(VMEM,) * 5,
+        scratch_shapes=[pltpu.VMEM(*entry) for entry in vmem]
+        + [dma(shape) for shape in sems]
+        + [dma, dma],
         compiler_params=pltpu.CompilerParams(
-            collective_id=1, has_side_effects=True, vmem_limit_bytes=24 << 20
+            collective_id=0, has_side_effects=True, vmem_limit_bytes=LIMIT << 20
         ),
-        name="combine",
+        name="whole",
         cost_estimate=pl.CostEstimate(
-            flops=2 * tokens * full * channels,
-            bytes_accessed=50 * partial_value.size * 2,
+            flops=18 * units * total * full,
+            bytes_accessed=200 * total * width * 2,
             transcendentals=0,
         ),
-    )(partial_value, cot, meta, proj, conv_out, row_mean, row_rstd, gain, taps, *acts)
+    )(*[pltpu.with_memory_space_constraint(value, pltpu.HBM) for value in operands])
+
+
+LIMIT = 40
 
 
 def finish_kernel(
@@ -995,8 +1061,7 @@
     taps,
     out_proj,
 ):
-    experts = lax.axis_size("sp")
-    expert_in, expert_cot, mixed_all, proj_all, meta = dispatch(
+    mine, unit_grad, columns, mixed_all, grads = whole(
         moe_input,
         cotangent,
         routes.T,
@@ -1006,34 +1071,11 @@
         row_rstd[None, :],
         ln_gain[None, :],
         out_proj,
-        experts,
-    )
-    gate_w = w_gate[0]
-    up_w = w_up[0]
-    down_w = w_down[0]
-    gate_pre = contract_cols(gate_w, expert_in)
-    up_pre = contract_cols(up_w, expert_in)
-    gate_sig = jax.nn.sigmoid(gate_pre)
-    gate_act = gate_pre * gate_sig
-    hidden = (gate_act * up_pre).astype(jnp.bfloat16)
-    hidden_grad = contract_cols(down_w, expert_cot)
-    gate_delta = (hidden_grad * up_pre * gate_sig * (1.0 + gate_pre * (1.0 - gate_sig))).astype(
-        jnp.bfloat16
-    )
-    up_delta = (hidden_grad * gate_act).astype(jnp.bfloat16)
-    partial_value = contract_rows(gate_delta, gate_w) + contract_rows(up_delta, up_w)
-    mine, unit_grad, columns, grads = combine(
-        partial_value.astype(jnp.bfloat16),
-        cotangent,
-        meta,
-        proj_all,
-        conv_out,
-        row_mean[None, :],
-        row_rstd[None, :],
-        ln_gain[None, :],
         taps,
-        (hidden, gate_delta, up_delta, expert_in, expert_cot),
-        experts,
+        w_gate,
+        w_up,
+        w_down,
+        lax.axis_size("sp"),
     )
     return finish(grads, mine, unit_grad, columns, mixed_all, cotangent, v_value, v_gate)
 
@@ -1042,7 +1084,7 @@
     tokens, width = blocks[0].shape
     depth, channels = blocks[-1].shape
     experts = lax.axis_size("sp")
-    square = lax.axis_size("tp") == 4 and experts % 2 == 0 and tokens == 128
+    square = lax.axis_size("tp") == 4 and experts % 8 == 0 and tokens == 128
     capacity = 4 * tokens // experts
     tiled = width % 128 == 0 and depth % 128 == 0 and channels % 128 == 0 and capacity % 16 == 0
     if square and tiled:

time: 109 us -> 101 us (0.927)
  the two profiles are of different devices: /device:TPU:9 before, /device:TPU:0 now
where the time goes in v3:
time: 101 us
  Pallas kernels  99.7 us (99%)
    pallas_call x1, Pallas kernels, whole(): pl.pallas_call(functools.partial(whole_kernel, count), out_shape=(jax.Sha...  96 us
    pallas_call x1, Pallas kernels, finish(): pl.pallas_call(finish_kernel, out_shape=tuple((jax.ShapeDtypeStruct(shape...  3.73 us

profile of v3, /device:TPU:0, one launch (start us, length us, event | category | flops | bytes accessed | tf_op | source)
XLA Modules:
  0.0 100.6 jit_solution(12382491830616786034)
XLA Ops:
  0.6 0.0 copy-start
  0.6 0.0 copy-start.1
  0.7 0.0 copy-start.2
  0.7 96.0 %whole.1 = (f32[128,512]{1,0:T(8,128)S(1)}, f32[128,256]{1,0:T(8,128)S(1)}, bf16[1024,256]{1,0:T(8,128)(2,1)S(1)}, bf16[1024,256]{1,0:T(8,128)(2,1)S(1)}, bf16[3,704,2048]{2,1,0:T(8,128)(2,1)S(1)}) custom-call(bf16[128,512]{1,0:T(8,128)(2,1)} %x.1, bf16[128,512]{1,0:T(8,128)(2,1)} %cot.3, s32[2,128]{1,0:T(2,128)} %bitcast.5, f32[2,128]{1,0:T(2,128)} %bitcast.6, ...), custom_call_target="tpu_custom_call" | custom-call | flops 13287555072 | bytes 104857600 | tf_op jit(solution)/shard_map/whole/pallas_call | solution.py:932
  96.7 0.0 copy-done
  96.7 0.0 copy-done.1
  96.7 0.0 copy-done.2
  96.7 3.7 %finish.1 = (bf16[1,704,2048]{2,1,0:T(8,128)(2,1)}, bf16[1,704,2048]{2,1,0:T(8,128)(2,1)}, bf16[1,704,2048]{2,1,0:T(8,128)(2,1)}, f32[256,256]{1,0:T(8,128)}, bf...) custom-call(bf16[3,704,2048]{2,1,0:T(8,128)(2,1)S(1)} %get-tuple-element.12.grads, ...), custom_call_target="tpu_custom_call" | custom-call | flops 134217728 | bytes 17301504 | tf_op jit(solution)/shard_map/finish/pallas_call | solution.py:1019
Async XLA Ops:
  0.6 96.0 %copy-start = (bf16[128,512]{1,0:T(8,128)(2,1)S(1)}, bf16[128,512]{1,0:T(8,128)(2,1)}, u32[]{:S(2)}) copy-start(bf16[128,512]{1,0:T(8,128)(2,1)} %cot.3) | copy-start | bytes 393220
  0.6 96.0 %copy-start.1 = (bf16[128,256]{1,0:T(8,128)(2,1)S(1)}, bf16[128,256]{1,0:T(8,128)(2,1)}, u32[]{:S(2)}) copy-start(bf16[128,256]{1,0:T(8,128)(2,1)} %v_value.1) | copy-start | bytes 196612
  0.7 96.0 %copy-start.2 = (bf16[128,256]{1,0:T(8,128)(2,1)S(1)}, bf16[128,256]{1,0:T(8,128)(2,1)}, u32[]{:S(2)}) copy-start(bf16[128,256]{1,0:T(8,128)(2,1)} %v_gate.1) | copy-start | bytes 196612

commit v4 on v3

--- a/solution.py
+++ b/solution.py
@@ -433,9 +433,8 @@
             meta, metas.at[me], meta_send.at[target], meta_recv.at[me], target, tp
         )
 
-    early = list(range(chips // 2))
-    late = list(range(chips // 2, chips))
-    line = [(a, j) for j in early for a in range(2)] + [(a, j) for a in range(2) for j in late]
+    line = [(a, j) for j in range(chips) for a in range(2)]
+    seats = list(range(1, chips)) + [0]
     blocks = len(line)
 
     def plane(j):
@@ -487,56 +486,51 @@
 
     def gather_rows(k):
         a, o = at(k)
-        j = line[k][1]
-        compact(a, 2 * o + lane, 2 * j)
+        seat = 2 * seats.index(line[k][1])
+        compact(a, 2 * o + lane, seat + 1)
         for q in range(5):
             push_copy(a, o, q, 1 - lane).wait_recv()
-        compact(a, 2 * o + 1 - lane, 2 * j + 1)
-
-    batch = rows.shape[0] // 2
-    tiles = 1
-    tile = units // tiles
-    breadth = 512 if width % 512 == 0 else width
+        compact(a, 2 * o + 1 - lane, seat)
+
+    small = 2 * capacity
+    lower_size = rows.shape[0] - 2 * small
+    own_start = rows.shape[0] - small
+    breadth = BREADTH if width % BREADTH == 0 else width
     pieces = 4 * width // breadth
 
-    def activate(h):
-        span = pl.ds(h * batch, batch)
-
-        def step(t, carry):
-            u = pl.ds(pl.multiple_of(t * tile, 16), tile)
-            gate = contract_cols(gate_w[u, :], rows[span, :])
-            up = contract_cols(up_w[u, :], rows[span, :])
-            gate_sig = jax.nn.sigmoid(gate)
-            gate_act = gate * gate_sig
-            hidden[u, span] = (gate_act * up).astype(jnp.bfloat16)
-            first_factor[u, :] = up * gate_sig * (1.0 + gate * (1.0 - gate_sig))
-            second_factor[u, :] = gate_act
-            return carry
-
-        lax.fori_loop(0, tiles, step, 0)
-
-    def deltas(h):
-        span = pl.ds(h * batch, batch)
-
-        def step(t, carry):
-            u = pl.ds(pl.multiple_of(t * tile, 16), tile)
-            hidden_grad = contract_cols(down_w[u, :], cots[span, :])
-            gate_delta[u, span] = (hidden_grad * first_factor[u, :]).astype(jnp.bfloat16)
-            up_delta[u, span] = (hidden_grad * second_factor[u, :]).astype(jnp.bfloat16)
-            return carry
-
-        lax.fori_loop(0, tiles, step, 0)
-        turned[0] = gate_delta[:, span].T
-        turned[1] = up_delta[:, span].T
-
-    def partials(h, first_piece, last_piece):
-        span = pl.ds(h * batch, batch)
+    def spans(start, size):
+        return pl.ds(start, size), pl.ds(start, size)
+
+    def activate(start, size):
+        span, local = spans(start, size)
+        gate = contract_cols(gate_w[...], rows[span, :])
+        up = contract_cols(up_w[...], rows[span, :])
+        gate_sig = jax.nn.sigmoid(gate)
+        gate_act = gate * gate_sig
+        hidden[:, span] = (gate_act * up).astype(jnp.bfloat16)
+        first_factor[:, local] = up * gate_sig * (1.0 + gate * (1.0 - gate_sig))
+        second_factor[:, local] = gate_act
+
+    def deltas(start, size):
+        span, local = spans(start, size)
+        hidden_grad = contract_cols(down_w[...], cots[span, :])
+        for index, (delta, factor) in enumerate(
+            ((gate_delta, first_factor), (up_delta, second_factor))
+        ):
+            value = (hidden_grad * factor[:, local]).astype(jnp.bfloat16)
+            delta[:, span] = value
+            turned[index, local] = value.T
+
+    def partials(start, size, first_piece, last_piece):
+        span, local = spans(start, size)
 
         def step(t, carry):
             spots = pl.ds(pl.multiple_of(t * breadth, 128), breadth)
-            value = jnp.dot(turned[0], gate_w[:, spots], preferred_element_type=jnp.float32)
+            value = jnp.dot(
+                turned[0, local, :], gate_w[:, spots], preferred_element_type=jnp.float32
+            )
             value = value + jnp.dot(
-                turned[1], up_w[:, spots], preferred_element_type=jnp.float32
+                turned[1, local, :], up_w[:, spots], preferred_element_type=jnp.float32
             )
             partial_ref[span, spots] = value.astype(jnp.bfloat16)
             return carry
@@ -559,7 +553,7 @@
         ]
 
     def source_of(step):
-        return 2 * plane(step // 2) + (lane if step % 2 == 0 else 1 - lane)
+        return 2 * plane(seats[step // 2]) + (1 - lane if step % 2 == 0 else lane)
 
     def near_far(step):
         return (across, down) if step % 2 == 0 else (down, across)
@@ -601,7 +595,7 @@
             for step in steps:
                 share_copy(step, q).start()
 
-    half_count = count // 2
+    half_count = count - 4
     lower, upper = range(half_count), range(half_count, count)
 
     def forward(step):
@@ -616,7 +610,7 @@
         total = share(step, tp)[...].astype(jnp.float32)
         total = total + landed[0, step].astype(jnp.float32)
         total = (total + landed[2, step].astype(jnp.float32)).astype(jnp.bfloat16)
-        if step > 0:
+        if step < count - 1:
             reduced[step] = total
             back_copy(step).start()
         else:
@@ -659,35 +653,39 @@
             corners(n - 1)
         if 2 <= n:
             gather_rows(n - 2)
-        if n == chips:
+        if n == 2:
             for copy in loads[-3:]:
                 copy.wait()
-            activate(0)
-        if n == chips + 1:
-            deltas(0)
-        if n == chips + 2:
-            partials(0, 0, pieces)
-        if n == chips + chips // 2 + 1:
-            activate(1)
+            activate(own_start, small)
+        if n == 3:
+            deltas(own_start, small)
+        if n == 4:
+            partials(own_start, small, 0, pieces)
+        if n == blocks - 2:
+            activate(0, lower_size)
         if n == blocks - 1:
+            begin(upper[-2:])
+            deltas(0, lower_size)
+            partials(0, lower_size, 0, pieces)
             begin(lower)
         if n == blocks:
-            forward(0)
+            activate(lower_size, small)
     slots_all = lax.broadcasted_iota(jnp.int32, (count * capacity, tokens), 0)
     slots_all = slots_all.astype(jnp.float32)
-    deltas(1)
-    for step in lower[1:]:
-        partials(1, pieces * (step - 1) // (half_count - 1), pieces * step // (half_count - 1))
-        if step == half_count - 1:
-            begin(upper)
+    deltas(lower_size, small)
+    forward(0)
+    forward(1)
+    settle(0)
+    partials(lower_size, small, 0, pieces)
+    begin(upper[:-2])
+    for step in lower[2:]:
         forward(step)
         settle(step - 1)
-    lax.fori_loop(0, pieces // 4, product, 0)
-    settle(half_count - 1)
+    quart = pieces // 4
+    lax.fori_loop(0, quart, product, 0)
     for step in upper:
         forward(step)
-        if step == half_count + 1:
-            lax.fori_loop(pieces // 4, pieces // 2, product, 0)
+        settle(step - 1)
     pick = jnp.where((meta[0:1, :] == slots_all) | (meta[1:2, :] == slots_all), 1.0, 0.0)
     pick = pick.astype(jnp.bfloat16)
     rstd = jnp.broadcast_to(row_rstd[...], (tokens, tokens)).T[:, 0:1]
@@ -696,9 +694,8 @@
     scaled = normed * gain[...]
     sig = jax.nn.sigmoid(scaled)
     slope = sig * (1.0 + scaled * (1.0 - sig)) * gain[...]
-    for step in upper:
-        settle(step)
-    lax.fori_loop(pieces // 2, 3 * pieces // 4, product, 0)
+    settle(count - 1)
+    lax.fori_loop(quart, 2 * quart, product, 0)
     for other in others:
         meta_copy(other).wait_send()
     for k in range(blocks):
@@ -740,7 +737,7 @@
 
     for q in range(3):
         wide_copy(q).start()
-    lax.fori_loop(3 * pieces // 4, pieces, product, 0)
+    lax.fori_loop(2 * quart, pieces, product, 0)
 
     def share_of(index):
         return jnp.dot(
@@ -867,7 +864,7 @@
         share_copy(step, 0).wait_send()
         share_copy(step, 1).wait_send()
         middle_copy(step).wait_send()
-    for step in range(1, count):
+    for step in range(count - 1):
         back_copy(step).wait_send()
     for other in others:
         strip_copy(other).wait_send()
@@ -910,9 +907,9 @@
         ((units, total), bf16),
         ((units, total), bf16),
         ((units, total), bf16),
-        ((units, total // 2), f32),
-        ((units, total // 2), f32),
-        ((2, total // 2, units), bf16),
+        ((units, total), f32),
+        ((units, total), f32),
+        ((2, total, units), bf16),
         ((total, full), bf16),
         ((3, count, capacity, width), bf16),
         ((count, capacity, width), bf16),
@@ -955,7 +952,8 @@
     )(*[pltpu.with_memory_space_constraint(value, pltpu.HBM) for value in operands])
 
 
-LIMIT = 40
+LIMIT = 42
+BREADTH = 512
 
 
 def finish_kernel(

time: 101 us -> 98.2 us (0.972)
  Pallas kernels: 99.7 us -> 97.2 us
    pallas_call x1, Pallas kernels: 96 us -> 93.4 us  [whole(): pl.pallas_call(functools.partial(whole_kernel, count), out_shape=(jax.Sha...]
where the time goes in v4:
time: 98.2 us; the launch traced here: 98 us
  Pallas kernels  97.2 us (99%)
    pallas_call x1, Pallas kernels, whole(): pl.pallas_call(functools.partial(whole_kernel, count), out_shape=(jax.Sha...  93.4 us
    pallas_call x1, Pallas kernels, finish(): pl.pallas_call(finish_kernel, out_shape=tuple((jax.ShapeDtypeStruct(shape...  3.73 us

profile of v4, /device:TPU:0, one launch (start us, length us, event | category | flops | bytes accessed | tf_op | source)
XLA Modules:
  0.0 98.0 jit_solution(4231228453442093165)
XLA Ops:
  0.6 0.0 copy-start
  0.6 0.0 copy-start.1
  0.7 0.0 copy-start.2
  0.7 93.4 %whole.1 = (f32[128,512]{1,0:T(8,128)S(1)}, f32[128,256]{1,0:T(8,128)S(1)}, bf16[1024,256]{1,0:T(8,128)(2,1)S(1)}, bf16[1024,256]{1,0:T(8,128)(2,1)S(1)}, bf16[3,704,2048]{2,1,0:T(8,128)(2,1)S(1)}) custom-call(bf16[128,512]{1,0:T(8,128)(2,1)} %x.1, bf16[128,512]{1,0:T(8,128)(2,1)} %cot.3, s32[2,128]{1,0:T(2,128)} %bitcast.5, f32[2,128]{1,0:T(2,128)} %bitcast.6, ...), custom_call_target="tpu_custom_call" | custom-call | flops 13287555072 | bytes 104857600 | tf_op jit(solution)/shard_map/whole/pallas_call | solution.py:929
  94.1 0.0 copy-done
  94.1 0.0 copy-done.1
  94.1 0.0 copy-done.2
  94.1 3.7 %finish.1 = (bf16[1,704,2048]{2,1,0:T(8,128)(2,1)}, bf16[1,704,2048]{2,1,0:T(8,128)(2,1)}, bf16[1,704,2048]{2,1,0:T(8,128)(2,1)}, f32[256,256]{1,0:T(8,128)}, bf...) custom-call(bf16[3,704,2048]{2,1,0:T(8,128)(2,1)S(1)} %get-tuple-element.12.grads, ...), custom_call_target="tpu_custom_call" | custom-call | flops 134217728 | bytes 17301504 | tf_op jit(solution)/shard_map/finish/pallas_call | solution.py:1017
Async XLA Ops:
  0.6 93.5 %copy-start = (bf16[128,512]{1,0:T(8,128)(2,1)S(1)}, bf16[128,512]{1,0:T(8,128)(2,1)}, u32[]{:S(2)}) copy-start(bf16[128,512]{1,0:T(8,128)(2,1)} %cot.3) | copy-start | bytes 393220
  0.6 93.5 %copy-start.1 = (bf16[128,256]{1,0:T(8,128)(2,1)S(1)}, bf16[128,256]{1,0:T(8,128)(2,1)}, u32[]{:S(2)}) copy-start(bf16[128,256]{1,0:T(8,128)(2,1)} %v_value.1) | copy-start | bytes 196612
  0.7 93.5 %copy-start.2 = (bf16[128,256]{1,0:T(8,128)(2,1)S(1)}, bf16[128,256]{1,0:T(8,128)(2,1)}, u32[]{:S(2)}) copy-start(bf16[128,256]{1,0:T(8,128)(2,1)} %v_gate.1) | copy-start | bytes 196612
